TPU v7x, 32 devices: a whole 2x2x4 slice. The times are simulated.
32 devices in a mesh: sp: 8 (over z, x), tp: 4 (over y, core).
Axes of the slice: x: 2, y: 2, z: 4, core: 2. Of those that a mesh axis runs over, the one named last changes fastest.
Arguments:
- tokens: bfloat16 [8192, 2048], P('sp', 'tp'), may hold values from -70 to 70
- w_query: bfloat16 [2048, 1024], P(None, 'tp'), may hold values from -0.125 to 0.125
- w_key: bfloat16 [2048, 1024], P(None, 'tp'), may hold values from -0.125 to 0.125
- w_value: bfloat16 [2048, 1024], P(None, 'tp'), may hold values from -0.125 to 0.125
- w_delta_gate: bfloat16 [2048, 1024], P(None, 'tp'), may hold values from -0.125 to 0.125
- w_glu_value: bfloat16 [2048, 1024], P(None, 'tp'), may hold values from -0.125 to 0.125
- w_glu_gate: bfloat16 [2048, 1024], P(None, 'tp'), may hold values from -0.125 to 0.125
- w_conv_gate: bfloat16 [2048, 1024], P(None, 'tp'), may hold values from -0.125 to 0.125
- w_beta: bfloat16 [2048, 8], replicated, may hold values from -0.125 to 0.125
- w_decay: bfloat16 [2048, 8], replicated, may hold values from -0.125 to 0.125
- decay_log: float32 [8], replicated, may hold values from -12 to -3
- head_gain: float32 [128], replicated, may hold values from 0.1 to 1.9
- conv_taps: bfloat16 [31, 1024], P(None, 'tp'), may hold values from -2.5 to 2.5
- ln_gain: float32 [1024], P('tp'), may hold values from 0.1 to 1.9
- ln_shift: float32 [1024], P('tp'), may hold values from -3 to 3
- out_delta: bfloat16 [1024, 2048], P('tp'), may hold values from -0.125 to 0.125
- out_conv: bfloat16 [1024, 2048], P('tp'), may hold values from -0.125 to 0.125
Outputs:
- mixed_out: bfloat16 [8192, 2048], P(('sp', 'tp'))
All inputs are finite; a program needn't handle non-finite values.
Results may differ from a plain program's by a relative error of at most 0.024.
Values may be sent and summed in bfloat16 or wider, within the bound.
A program may use at most 64 MiB of HBM per device.

v0:
```python
import functools

import jax
import jax.numpy as jnp
from jax import lax
from jax.experimental import pallas as pl
from jax.experimental.pallas import tpu as pltpu
from jax.sharding import PartitionSpec as P

BLOCK = 128
CHUNKS = 8
TOGETHER = 8
CUTS = 8


TINY_NORM = 1e-06
TINY_VAR = 1e-05
HIGHEST = lax.Precision.HIGHEST


def nt(a, b):
    return lax.dot_general(a, b, (((1,), (1,)), ((), ())), preferred_element_type=jnp.float32)


def mm(a, b):
    return jnp.dot(
        a.astype(jnp.bfloat16), b.astype(jnp.bfloat16), preferred_element_type=jnp.float32
    )


def delta_kernel(
    heads, width, q_ref, k_ref, v_ref, g_ref, outa_ref, outb_ref, final_ref,
    lhs_s, corr_s, score_s, wt_s, tail_s, state_ref,
):
    rows = q_ref.shape[0]
    blocks = rows // BLOCK
    row_id = lax.broadcasted_iota(jnp.int32, (BLOCK, BLOCK), 0)
    col_id = lax.broadcasted_iota(jnp.int32, (BLOCK, BLOCK), 1)
    causal = row_id >= col_id
    strict = row_id > col_id
    differ = row_id ^ col_id
    eye = jnp.where(row_id == col_id, 1.0, 0.0)
    tril = jnp.where(causal, 1.0, 0.0)

    def prepare(c):
        at = pl.ds(pl.multiple_of(c * BLOCK, BLOCK), BLOCK)
        gates = g_ref[at, :]
        sums = jnp.dot(tril, gates, precision=HIGHEST, preferred_element_type=jnp.float32)
        chains = []
        for h in range(heads):
            lanes = slice(h * width, (h + 1) * width)
            k, q = k_ref[at, lanes], q_ref[at, lanes]
            v = v_ref[at, lanes].astype(jnp.float32)
            kf, qf = k.astype(jnp.float32), q.astype(jnp.float32)
            ik = lax.rsqrt(jnp.sum(kf * kf, axis=-1, keepdims=True) + TINY_NORM)
            iq = lax.rsqrt(jnp.sum(qf * qf, axis=-1, keepdims=True) + TINY_NORM)
            iq = iq * width ** (-0.5)
            beta = gates[:, h : h + 1]
            log_sum = sums[:, heads + h : heads + h + 1]
            log_full = jnp.broadcast_to(log_sum, (BLOCK, BLOCK))
            spread = log_full - log_full.T
            damp = jnp.where(causal, jnp.exp(jnp.where(causal, spread, 0.0)), 0.0)
            damp = damp * jnp.broadcast_to(ik, (BLOCK, BLOCK)).T
            lower = jnp.where(strict, nt(k, k) * damp * (beta * ik), 0.0)
            score_s[h, at, :] = (nt(q, k) * damp * iq).astype(jnp.bfloat16)
            grow = jnp.exp(log_sum)
            right = jnp.concatenate([v * beta, kf * (beta * ik * grow)], axis=1)
            tail = log_full[BLOCK - 1 : BLOCK, :]
            weighted = kf * (ik * jnp.exp(tail[:, :1] - log_sum))
            wt_s[h, c] = weighted.T.astype(jnp.bfloat16)
            tail_s[h, c] = jnp.broadcast_to(jnp.exp(tail), (8, BLOCK))
            lhs_s[h, c, BLOCK:, :] = (qf * (iq * grow)).astype(jnp.bfloat16)
            chains.append([h, lower, right, eye - jnp.where(differ == 1, lower, 0.0)])
        return at, c, chains

    def pair(p, carry):
        prepared = [prepare(p * TOGETHER + i) for i in range(TOGETHER)]
        size = 2
        while size < BLOCK:
            level = (differ >= size) & (differ < 2 * size)
            parts = [
                [mm(jnp.where(level, ch[1], 0.0), ch[3]) for ch in item[2]] for item in prepared
            ]
            for item, part in zip(prepared, parts):
                for ch, moved in zip(item[2], part):
                    ch[3] = ch[3] - mm(ch[3], moved)
            size *= 2
        for at, c, chains in prepared:
            for h, lower, right, inverse in chains:
                solved = mm(inverse, right)
                corr_s[h, at, :] = solved[:, :width]
                lhs_s[h, c, :BLOCK, :] = solved[:, width:].astype(jnp.bfloat16)
        return carry

    lax.fori_loop(0, blocks // TOGETHER, pair, 0)
    for h in range(heads):
        state_ref[h] = jnp.concatenate([eye, jnp.zeros((width, width), jnp.float32)], axis=1)

    def advance(c, carry):
        at = pl.ds(pl.multiple_of(c * BLOCK, BLOCK), BLOCK)
        boths = [mm(lhs_s[h, c], state_ref[h]) for h in range(heads)]
        fresh = []
        for h in range(heads):
            first = boths[h][:BLOCK]
            fresh.append(
                jnp.concatenate(
                    [-first[:, :width], corr_s[h, at, :] - first[:, width:]], axis=1
                ).astype(jnp.bfloat16)
            )
        for h in range(heads):
            decay = tail_s[h, c][:1, :]
            decay = jnp.concatenate([decay, decay], axis=1)
            state_ref[h] = state_ref[h] * decay + mm(wt_s[h, c], fresh[h])
        for h in range(heads):
            out = boths[h][BLOCK:] + mm(score_s[h, at, :], fresh[h])
            outa_ref[h, at, :] = out[:, :width].astype(jnp.bfloat16)
            outb_ref[h, at, :] = out[:, width:]
        return carry

    lax.fori_loop(0, blocks, advance, 0)
    final_ref[...] = state_ref[...].astype(jnp.bfloat16)


def delta_rule(query_raw, key_raw, value_raw, gates, heads, width):
    rows = query_raw.shape[0]
    blocks = rows // BLOCK
    vm = pl.BlockSpec(memory_space=pltpu.VMEM)
    return pl.pallas_call(
        functools.partial(delta_kernel, heads, width),
        out_shape=(
            jax.ShapeDtypeStruct((heads, rows, width), jnp.bfloat16),
            jax.ShapeDtypeStruct((heads, rows, width), jnp.float32),
            jax.ShapeDtypeStruct((heads, width, 2 * width), jnp.bfloat16),
        ),
        in_specs=[vm] * 4,
        out_specs=(vm, vm, vm),
        scratch_shapes=[
            pltpu.VMEM((heads, blocks, 2 * BLOCK, width), jnp.bfloat16),
            pltpu.VMEM((heads, rows, width), jnp.float32),
            pltpu.VMEM((heads, rows, BLOCK), jnp.bfloat16),
            pltpu.VMEM((heads, blocks, width, BLOCK), jnp.bfloat16),
            pltpu.VMEM((heads, blocks, 8, BLOCK), jnp.float32),
            pltpu.VMEM((heads, width, 2 * width), jnp.float32),
        ],
        compiler_params=pltpu.CompilerParams(
            vmem_limit_bytes=40 * 1024 * 1024
        ),
        cost_estimate=pl.CostEstimate(
            flops=10_000_000_000, bytes_accessed=4_000_000, transcendentals=0
        ),
        name="delta_rule",
    )(query_raw, key_raw, value_raw, gates)


MESH = pl.DeviceIdType.MESH


def sharded_place():
    tp = lax.axis_size("tp")
    me = lax.axis_index("tp")
    core = lax.rem(me, 2)
    return tp // 2, me, core, me // 2, me + 1 - 2 * core


def greet(chips, core, chip, sibling):
    barrier = pltpu.get_barrier_semaphore()
    pl.semaphore_signal(barrier, inc=1, device_id={"tp": sibling}, device_id_type=MESH)
    for o in range(1, chips):
        there = lax.rem(chip + o, chips) * 2 + core
        pl.semaphore_signal(barrier, inc=1, device_id={"tp": there}, device_id_type=MESH)
    pl.semaphore_wait(barrier, chips)


def project_kernel(heads, *refs):
    count = 7
    tok_ref, far_refs, wg_ref, rate_ref = refs[0], refs[1 : 1 + count], refs[8], refs[9]
    out_refs, gates_ref = refs[10 : 10 + count], refs[17]
    full, y_send, y_recv, own_send, own_recv, fwd_send, fwd_recv, w_sem = refs[18:26]
    w_refs = refs[26:]
    rows, part = tok_ref.shape
    step = rows // CHUNKS
    chips, me, core, chip, sibling = sharded_place()

    def columns(owner):
        return pl.ds(pl.multiple_of(owner * part, part), part)

    def at(r):
        return pl.ds(pl.multiple_of(r * step, step), step)

    def across(o, r):
        there = lax.rem(chip + o, chips) * 2 + core
        return pltpu.make_async_remote_copy(
            src_ref=tok_ref.at[at(r), :],
            dst_ref=full.at[at(r), columns(me)],
            send_sem=y_send.at[o - 1, r],
            recv_sem=y_recv.at[o - 1, r],
            device_id={"tp": there},
            device_id_type=MESH,
        )

    def beside(r):
        return pltpu.make_async_remote_copy(
            src_ref=tok_ref.at[at(r), :],
            dst_ref=full.at[at(r), columns(me)],
            send_sem=own_send.at[r],
            recv_sem=own_recv.at[r],
            device_id={"tp": sibling},
            device_id_type=MESH,
        )

    def forward(o, r):
        owner = lax.rem(chip - o + chips, chips) * 2 + core
        block = full.at[at(r), columns(owner)]
        return pltpu.make_async_remote_copy(
            src_ref=block,
            dst_ref=block,
            send_sem=fwd_send.at[o - 1, r],
            recv_sem=fwd_recv.at[o - 1, r],
            device_id={"tp": sibling},
            device_id_type=MESH,
        )

    greet(chips, core, chip, sibling)
    for r in range(CHUNKS):
        for o in range(1, chips):
            across(o, r).start()
    loads = [
        pltpu.make_async_copy(far, w_ref, w_sem.at[i])
        for i, (far, w_ref) in enumerate(zip(far_refs, w_refs))
    ]
    for load in loads:
        load.start()
    for r in range(CHUNKS):
        beside(r).start()
    full[:, columns(me)] = tok_ref[...]

    def chunk(first, pieces, carry):
        for i in range(pieces):
            for o in range(1, chips):
                across(o, first + i).wait_recv()
                forward(o, first + i).start()
        for i in range(pieces):
            beside(first + i).wait_recv()
            for o in range(1, chips):
                forward(o, first + i).wait_recv()
        size = step * pieces
        here = pl.ds(pl.multiple_of(first * step, step), size)
        squares = jnp.zeros((size, 1), jnp.float32)
        for b in range(2 * chips):
            piece = full[here, b * part : (b + 1) * part].astype(jnp.float32)
            squares = squares + jnp.sum(piece * piece, axis=1, keepdims=True)
        inv_rms = lax.rsqrt(squares / (part * 2 * chips) + TINY_NORM)
        for w_ref, out_ref in zip(w_refs, out_refs):
            summed = jnp.dot(full[here, :], w_ref[...], preferred_element_type=jnp.float32)
            out_ref[here, :] = (summed * inv_rms).astype(jnp.bfloat16)
        raw = jnp.dot(full[here, :], wg_ref[...], preferred_element_type=jnp.float32) * inv_rms
        lane = lax.broadcasted_iota(jnp.int32, raw.shape, 1)
        softplus = jnp.maximum(raw, 0.0) + jnp.log1p(jnp.exp(-jnp.abs(raw)))
        gates_ref[here, :] = jnp.where(lane < heads, jax.nn.sigmoid(raw), -rate_ref[...] * softplus)
        return carry

    for load in loads:
        load.wait()
    paired = CHUNKS // 2 - 1
    lax.fori_loop(0, paired, lambda r, carry: chunk(2 * r, 2, carry), 0)
    lax.fori_loop(2 * paired, CHUNKS, lambda r, carry: chunk(r, 1, carry), 0)
    for r in range(CHUNKS):
        for o in range(1, chips):
            across(o, r).wait_send()
            forward(o, r).wait_send()
        beside(r).wait_send()


def project(tokens, weights, w_gates, rates, heads):
    rows, part = tokens.shape
    tp = lax.axis_size("tp")
    others = max(tp // 2 - 1, 1)
    vm = pl.BlockSpec(memory_space=pltpu.VMEM)
    dma = pltpu.SemaphoreType.DMA
    return pl.pallas_call(
        functools.partial(project_kernel, heads),
        out_shape=tuple(
            jax.ShapeDtypeStruct((rows, w.shape[1]), jnp.bfloat16) for w in weights
        )
        + (jax.ShapeDtypeStruct((rows, w_gates.shape[1]), jnp.float32),),
        in_specs=[vm] + [pl.BlockSpec(memory_space=pl.ANY)] * len(weights) + [vm] * 2,
        out_specs=(vm,) * (1 + len(weights)),
        scratch_shapes=[
            pltpu.VMEM((rows, part * tp), jnp.bfloat16),
            dma((others, CHUNKS)),
            dma((others, CHUNKS)),
            dma((CHUNKS,)),
            dma((CHUNKS,)),
            dma((others, CHUNKS)),
            dma((others, CHUNKS)),
            dma((len(weights),)),
        ]
        + [pltpu.VMEM(w.shape, w.dtype) for w in weights],
        compiler_params=pltpu.CompilerParams(
            collective_id=0, has_side_effects=True, vmem_limit_bytes=48 * 1024 * 1024
        ),
        cost_estimate=pl.CostEstimate(
            flops=10_000_000_000, bytes_accessed=20_000_000, transcendentals=0
        ),
        name="gather_project",
    )(tokens, *weights, w_gates, rates)


def middle_kernel(
    heads, width, final_ref, gv_ref, gg_ref, cg_ref, taps_ref, ln_gain_ref, ln_shift_ref,
    outa_ref, outb_ref, dg_ref, gain_ref, mixed_ref, conv_ref,
    padded, filtered, halo_out, halo_in, sums_out, sums_in, near, window_s, sent_s, far_s,
    near_send, near_recv, far_send, far_recv, halo_send, halo_recv, ln_send, ln_recv,
):
    rows = gv_ref.shape[0]
    halo = halo_in.shape[0]
    lanes = padded.shape[2]
    groups = padded.shape[0]
    kernel = taps_ref.shape[0]
    tiles = rows // BLOCK
    sp, place = lax.axis_size("sp"), lax.axis_index("sp")
    tp, me = lax.axis_size("tp"), lax.axis_index("tp")
    reaches = [2]
    while 2 * reaches[-1] < sp:
        reaches.append(2 * reaches[-1])
    distances = [1, 2] + reaches[1:]
    barrier = pltpu.get_barrier_semaphore()
    for step in distances:
        for to in (step, sp - step):
            pl.semaphore_signal(
                barrier, inc=1, device_id={"sp": lax.rem(place + to, sp)}, device_id_type=MESH
            )
    for step in range(1, tp):
        pl.semaphore_signal(
            barrier, inc=1, device_id={"tp": lax.rem(me + step, tp)}, device_id_type=MESH
        )
    pl.semaphore_wait(barrier, 2 * len(distances) + tp - 1)

    def onward(src, dst, send, recv, step):
        return pltpu.make_async_remote_copy(
            src_ref=src,
            dst_ref=dst,
            send_sem=send,
            recv_sem=recv,
            device_id={"sp": lax.rem(place + step, sp)},
            device_id_type=MESH,
        )

    firsts = [
        onward(final_ref, near.at[i], near_send.at[i], near_recv.at[i], i + 1) for i in range(2)
    ]
    for copy in firsts:
        copy.start()

    def at(t):
        return pl.ds(pl.multiple_of(t * BLOCK, BLOCK), BLOCK)

    def unit(t, carry):
        value = gv_ref[at(t), :].astype(jnp.float32)
        units = (value * jax.nn.sigmoid(gg_ref[at(t), :].astype(jnp.float32))).astype(jnp.bfloat16)
        wide = units.astype(jnp.float32)
        for g in range(groups):
            padded[g, pl.ds(pl.multiple_of(t * BLOCK + halo, halo), BLOCK), :] = wide[
                :, g * lanes : (g + 1) * lanes
            ]
        return units

    units = unit(tiles - 1, 0)
    halo_out[...] = units[BLOCK - halo :, :]
    halo_copy = onward(halo_out, halo_in, halo_send.at[0], halo_recv.at[0], 1)
    halo_copy.start()

    def unit_loop(t, carry):
        unit(t, 0)
        return carry

    lax.fori_loop(0, tiles - 1, unit_loop, 0)

    def conv(t, carry):
        first = jnp.zeros((BLOCK, 1), jnp.float32)
        second = jnp.zeros((BLOCK, 1), jnp.float32)
        for g in range(groups):
            total = jnp.zeros((BLOCK, lanes), jnp.float32)
            for j in range(kernel):
                start = t * BLOCK + (halo - kernel + 1 + j)
                tap = taps_ref[j : j + 1, g * lanes : (g + 1) * lanes]
                total = total + padded[g, pl.ds(start, BLOCK), :] * tap
            filtered[g, at(t), :] = total
            first = first + jnp.sum(total, axis=1, keepdims=True)
            second = second + jnp.sum(total * total, axis=1, keepdims=True)
        lane = lax.broadcasted_iota(jnp.int32, (BLOCK, BLOCK), 1)
        sums_out[t] = jnp.where(lane == 0, first, jnp.where(lane == 1, second, 0.0)).T[:8, :]
        return carry

    half = tiles // 2
    lax.fori_loop(1, half, conv, 0)
    for copy in firsts:
        copy.wait()
    for h in range(heads):
        one = jnp.where(place >= 1, near[0, h].astype(jnp.float32), 0.0)
        two = jnp.where(place >= 2, near[1, h].astype(jnp.float32), 0.0)
        moved = mm(one[:, :width], two)
        window_s[h] = jnp.concatenate(
            [moved[:, :width], moved[:, width:] + one[:, width:]], axis=1
        )
        sent_s[0, h] = window_s[h].astype(jnp.bfloat16)

    def step_copy(i):
        return onward(sent_s.at[i], far_s.at[i], far_send.at[i], far_recv.at[i], reaches[i])

    step_copy(0).start()
    lax.fori_loop(half, tiles, conv, 0)
    halo_copy.wait()
    before = jnp.where(place >= 1, halo_in[...].astype(jnp.float32), 0.0)
    for g in range(groups):
        padded[g, :halo, :] = before[:, g * lanes : (g + 1) * lanes]
    conv(0, 0)

    def ln_copy(step):
        return pltpu.make_async_remote_copy(
            src_ref=sums_out,
            dst_ref=sums_in.at[step - 1],
            send_sem=ln_send.at[step - 1],
            recv_sem=ln_recv.at[step - 1],
            device_id={"tp": lax.rem(me + step, tp)},
            device_id_type=MESH,
        )

    for step in range(1, tp):
        ln_copy(step).start()
    for i in range(len(reaches) - 1):
        step_copy(i).wait()
        for h in range(heads):
            earlier = jnp.where(place >= reaches[i], far_s[i, h].astype(jnp.float32), 0.0)
            window = window_s[h]
            moved = mm(window[:, :width], earlier)
            window_s[h] = jnp.concatenate(
                [moved[:, :width], moved[:, width:] + window[:, width:]], axis=1
            )
            sent_s[i + 1, h] = window_s[h].astype(jnp.bfloat16)
        step_copy(i + 1).start()
    for step in range(1, tp):
        ln_copy(step).wait()
    channels = groups * lanes * tp

    def norm(t, carry):
        sums = sums_out[t]
        for step in range(1, tp):
            sums = sums + sums_in[step - 1, t]
        sums = jnp.concatenate([sums, jnp.zeros((BLOCK - 8, BLOCK), jnp.float32)], axis=0).T
        center = sums[:, 0:1] / channels
        variance = jnp.maximum(sums[:, 1:2] / channels - center * center, 0.0)
        scale = lax.rsqrt(variance + TINY_VAR)
        for g in range(groups):
            cut = slice(g * lanes, (g + 1) * lanes)
            normed = (filtered[g, at(t), :] - center) * scale
            normed = normed * ln_gain_ref[:, cut] + ln_shift_ref[:, cut]
            gate = cg_ref[at(t), cut].astype(jnp.float32)
            conv_ref[at(t), cut] = (jax.nn.silu(normed) * jax.nn.silu(gate)).astype(jnp.bfloat16)
        return carry

    lax.fori_loop(0, tiles, norm, 0)
    last = len(reaches) - 1
    step_copy(last).wait()
    carried = []
    for h in range(heads):
        earlier = jnp.where(
            place >= reaches[last], far_s[last, h, :, width:].astype(jnp.float32), 0.0
        )
        window = window_s[h]
        carried.append((mm(window[:, :width], earlier) + window[:, width:]).astype(jnp.bfloat16))

    def one_tile(t, carry):
        for h in range(heads):
            cut = slice(h * width, (h + 1) * width)
            result = outb_ref[h, at(t), :] + mm(outa_ref[h, at(t), :], carried[h])
            result = result * lax.rsqrt(
                jnp.mean(result * result, axis=-1, keepdims=True) + TINY_NORM
            )
            gate = dg_ref[at(t), cut].astype(jnp.float32)
            mixed_ref[at(t), cut] = (result * gain_ref[...] * jax.nn.silu(gate)).astype(
                jnp.bfloat16
            )
        return carry

    lax.fori_loop(0, tiles, one_tile, 0)


def middle(final, glu_value, glu_gate, conv_gate, taps, ln_gain, ln_shift, outa, outb, gate, gain):
    heads, width = final.shape[0], final.shape[1]
    rows, channels = glu_value.shape
    kernel = taps.shape[0]
    halo = (kernel - 1 + 31) // 32 * 32
    lanes = min(channels, 128)
    groups = channels // lanes
    sp, tp = lax.axis_size("sp"), lax.axis_size("tp")
    steps = 1
    while 2 ** (steps + 1) < sp:
        steps += 1
    vm = pl.BlockSpec(memory_space=pltpu.VMEM)
    dma = pltpu.SemaphoreType.DMA
    tiles = rows // BLOCK
    pair = (heads, width, 2 * width)
    return pl.pallas_call(
        functools.partial(middle_kernel, heads, width),
        out_shape=(
            jax.ShapeDtypeStruct((rows, heads * width), jnp.bfloat16),
            jax.ShapeDtypeStruct((rows, channels), jnp.bfloat16),
        ),
        in_specs=[vm] * 11,
        out_specs=(vm, vm),
        scratch_shapes=[
            pltpu.VMEM((groups, halo + rows, lanes), jnp.float32),
            pltpu.VMEM((groups, rows, lanes), jnp.float32),
            pltpu.VMEM((halo, channels), jnp.bfloat16),
            pltpu.VMEM((halo, channels), jnp.bfloat16),
            pltpu.VMEM((tiles, 8, BLOCK), jnp.float32),
            pltpu.VMEM((tp - 1, tiles, 8, BLOCK), jnp.float32),
            pltpu.VMEM((2,) + pair, jnp.bfloat16),
            pltpu.VMEM(pair, jnp.float32),
            pltpu.VMEM((steps,) + pair, jnp.bfloat16),
            pltpu.VMEM((steps,) + pair, jnp.bfloat16),
            dma((2,)),
            dma((2,)),
            dma((steps,)),
            dma((steps,)),
            dma((1,)),
            dma((1,)),
            dma((tp - 1,)),
            dma((tp - 1,)),
        ],
        compiler_params=pltpu.CompilerParams(
            collective_id=2, has_side_effects=True, vmem_limit_bytes=40 * 1024 * 1024
        ),
        cost_estimate=pl.CostEstimate(
            flops=10_000_000_000, bytes_accessed=20_000_000, transcendentals=0
        ),
        name="exchange_middle",
    )(final, glu_value, glu_gate, conv_gate, taps, ln_gain, ln_shift, outa, outb, gate, gain)


def output_kernel(
    dm_ref, cm_ref, wd_ref, wc_ref, out_ref,
    beside_out, beside_in, across_out, across_in, b_send, b_recv, y_send, y_recv,
):
    chips, me, core, chip, sibling = sharded_place()
    rows = out_ref.shape[0]
    width = out_ref.shape[1] // CUTS

    def cols(n):
        return pl.ds(pl.multiple_of(n * width, width), width)

    def partial(target, n):
        at = pl.ds(pl.multiple_of(target * rows, rows), rows)
        summed = jnp.dot(dm_ref[at, :], wd_ref[:, cols(n)], preferred_element_type=jnp.float32)
        return summed + jnp.dot(
            cm_ref[at, :], wc_ref[:, cols(n)], preferred_element_type=jnp.float32
        )

    def beside(o, n):
        return pltpu.make_async_remote_copy(
            src_ref=beside_out.at[o, n],
            dst_ref=beside_in.at[o, n],
            send_sem=b_send.at[o, n],
            recv_sem=b_recv.at[o, n],
            device_id={"tp": sibling},
            device_id_type=MESH,
        )

    def across(o, n):
        there = lax.rem(chip + o, chips) * 2 + core
        return pltpu.make_async_remote_copy(
            src_ref=across_out.at[o - 1, n],
            dst_ref=across_in.at[o - 1, n],
            send_sem=y_send.at[o - 1, n],
            recv_sem=y_recv.at[o - 1, n],
            device_id={"tp": there},
            device_id_type=MESH,
        )

    greet(chips, core, chip, sibling)
    order = list(range(1, chips)) + [0]
    for o in order:
        their_chip = lax.rem(chip + o, chips) * 2

        def give(n, carry, o=o, their_chip=their_chip):
            beside_out[o, n] = partial(their_chip + 1 - core, n).astype(jnp.bfloat16)
            beside(o, n).start()
            return carry

        def keep(n, carry, o=o, their_chip=their_chip):
            mine = partial(their_chip + core, n)
            beside(o, n).wait_recv()
            mine = mine + beside_in[o, n].astype(jnp.float32)
            across_out[o - 1, n] = mine.astype(jnp.bfloat16)
            across(o, n).start()
            return carry

        if o != 0:

            def both(n, carry, give=give, keep=keep):
                @pl.when(n + 1 < CUTS)
                def _():
                    give(n + 1, 0)

                return keep(n, carry)

            give(0, 0)
            lax.fori_loop(0, CUTS, both, 0)
        else:
            lax.fori_loop(0, CUTS, give, 0)

    def close(n, carry):
        mine = partial(me, n)
        beside(0, n).wait_recv()
        mine = mine + beside_in[0, n].astype(jnp.float32)
        for o in range(1, chips):
            across(o, n).wait_recv()
            mine = mine + across_in[o - 1, n].astype(jnp.float32)
        out_ref[:, cols(n)] = mine.astype(jnp.bfloat16)
        return carry

    lax.fori_loop(0, CUTS, close, 0)

    def drain(n, carry):
        for o in range(chips):
            beside(o, n).wait_send()
        for o in range(1, chips):
            across(o, n).wait_send()
        return carry

    lax.fori_loop(0, CUTS, drain, 0)


def output_projection(delta_mixed, conv_mixed, out_delta, out_conv):
    tp = lax.axis_size("tp")
    chips = tp // 2
    others = max(chips - 1, 1)
    rows = delta_mixed.shape[0] // tp
    width = out_delta.shape[1]
    cut = width // CUTS
    vm = pl.BlockSpec(memory_space=pltpu.VMEM)
    dma = pltpu.SemaphoreType.DMA
    return pl.pallas_call(
        output_kernel,
        out_shape=jax.ShapeDtypeStruct((rows, width), jnp.bfloat16),
        in_specs=[vm] * 4,
        out_specs=vm,
        scratch_shapes=[
            pltpu.VMEM((chips, CUTS, rows, cut), jnp.bfloat16),
            pltpu.VMEM((chips, CUTS, rows, cut), jnp.bfloat16),
            pltpu.VMEM((others, CUTS, rows, cut), jnp.bfloat16),
            pltpu.VMEM((others, CUTS, rows, cut), jnp.bfloat16),
            dma((chips, CUTS)),
            dma((chips, CUTS)),
            dma((others, CUTS)),
            dma((others, CUTS)),
        ],
        compiler_params=pltpu.CompilerParams(
            collective_id=1, has_side_effects=True, vmem_limit_bytes=48 * 1024 * 1024
        ),
        cost_estimate=pl.CostEstimate(
            flops=10_000_000_000, bytes_accessed=20_000_000, transcendentals=0
        ),
        name="output_scatter",
    )(delta_mixed, conv_mixed, out_delta, out_conv)


def local(
    tokens,
    w_query,
    w_key,
    w_value,
    w_delta_gate,
    w_glu_value,
    w_glu_gate,
    w_conv_gate,
    w_beta,
    w_decay,
    decay_log,
    head_gain,
    conv_taps,
    ln_gain,
    ln_shift,
    out_delta,
    out_conv,
):
    head_size = head_gain.shape[0]
    heads_here = w_query.shape[1] // head_size
    first_head = lax.axis_index("tp") * heads_here
    rates = jnp.exp(lax.dynamic_slice_in_dim(decay_log, first_head, heads_here, 0))
    fill = head_size - 2 * heads_here
    rates = jnp.concatenate(
        [jnp.zeros((heads_here,), jnp.float32), rates, jnp.zeros((fill,), jnp.float32)]
    )[None, :]
    w_gates = jnp.concatenate(
        [
            lax.dynamic_slice_in_dim(w_beta, first_head, heads_here, 1),
            lax.dynamic_slice_in_dim(w_decay, first_head, heads_here, 1),
            jnp.zeros((w_beta.shape[0], fill), jnp.bfloat16),
        ],
        axis=1,
    )
    weights = (w_query, w_key, w_value, w_delta_gate, w_glu_value, w_glu_gate, w_conv_gate)
    (
        query_raw,
        key_raw,
        value_raw,
        delta_gate_raw,
        glu_value_raw,
        glu_gate_raw,
        conv_gate_raw,
        gates,
    ) = project(tokens, weights, w_gates, rates, heads_here)
    outa, outb, final = delta_rule(
        query_raw, key_raw, value_raw, gates, heads_here, head_size
    )
    delta_mixed, conv_mixed = middle(
        final,
        glu_value_raw,
        glu_gate_raw,
        conv_gate_raw,
        conv_taps.astype(jnp.float32),
        ln_gain[None, :],
        ln_shift[None, :],
        outa,
        outb,
        delta_gate_raw,
        head_gain[None, :],
    )
    return output_projection(delta_mixed, conv_mixed, out_delta, out_conv)


def solution(mesh):
    return jax.shard_map(
        local,
        mesh=mesh,
        in_specs=(
            P("sp", "tp"),
            P(None, "tp"),
            P(None, "tp"),
            P(None, "tp"),
            P(None, "tp"),
            P(None, "tp"),
            P(None, "tp"),
            P(None, "tp"),
            P(),
            P(),
            P(),
            P(),
            P(None, "tp"),
            P("tp"),
            P("tp"),
            P("tp", None),
            P("tp", None),
        ),
        out_specs=P(("sp", "tp"), None),
        check_vma=False,
    )
```

profile of v0, /device:TPU:7, one launch (start us, length us, event | category | flops | bytes accessed | tf_op | source)
XLA Modules:
  0.0 95.5 jit_solution(15159123228348036131)
XLA Ops:
  0.0 0.8 constant_dynamic-slice_fusion
  0.8 0.3 copy.20
  1.1 0.0 copy-start
  1.1 0.3 copy.21
  1.4 0.1 pad.5.clone
  1.5 0.3 maximum_maximum_fusion.refs_8_
  1.9 0.3 copy-done.7
  2.2 0.1 dynamic-slice_exponential_fusion
  2.3 0.1 maximum_bitcast_fusion.refs_9_
  2.3 0.0 copy-done
  2.3 29.6 %gather_project.1 = (bf16[1024,256]{1,0:T(8,128)(2,1)S(1)}, bf16[1024,256]{1,0:T(8,128)(2,1)S(1)}, bf16[1024,256]{1,0:T(8,128)(2,1)S(1)}, bf16[1024,256]{1,0:T(8...) custom-call(bf16[1024,512]{1,0:T(8,128)(2,1)S(1)} %copy-done, ...), custom_call_target="tpu_custom_call" | custom-call | flops 10000000000 | bytes 20000000 | tf_op jit(solution)/shard_map/gather_project/pallas_call | solution.py:280
  32.0 0.0 copy-start.6
  32.0 0.0 copy-start.4
  32.0 8.6 %delta_rule.1 = (bf16[2,1024,128]{2,1,0:T(8,128)(2,1)S(1)}, f32[2,1024,128]{2,1,0:T(8,128)S(1)}, bf16[2,128,256]{2,1,0:T(8,128)(2,1)S(1)}) custom-call(bf16[1024,256]{1,0:T(8,128)(2,1)S(1)} %get-tuple-element.18.q_ref, bf16[1024,256]{1,0:T(8,128)(2,1)S(1)} %get-tuple-element.19.k_ref, bf16[1024,256]{1,0:T(8,128)(2,1)S(1)} %get-tuple-element.20.v_ref, ...), custom_call_target="tpu_custom_call" | custom-call | flops 10000000000 | bytes 4000000 | tf_op jit(solution)/shard_map/delta_rule/pallas_call | solution.py:128
  40.6 0.0 copy-done.6
  40.6 0.0 copy-start.3
  40.6 0.0 copy-start.5
  40.7 0.6 copy-done.3
  41.3 0.0 copy-done.5
  41.3 25.7 %exchange_middle.1 = (bf16[1024,256]{1,0:T(8,128)(2,1)S(1)}, bf16[1024,256]{1,0:T(8,128)(2,1)S(1)}) custom-call(bf16[2,128,256]{2,1,0:T(8,128)(2,1)S(1)} %get-tuple-element.22.final_ref, bf16[1024,256]{1,0:T(8,128)(2,1)S(1)} %get-tuple-element.23.gv_ref, bf16[1024,256]{1,0:T(8,128)(2,1)S(1)} %get-tuple-element.24.gg_ref, ...), custom_call_target="tpu_custom_call" | custom-call | flops 10000000000 | bytes 20000000 | tf_op jit(solution)/shard_map/exchange_middle/pallas_call | solution.py:504
  67.0 0.0 copy-done.1
  67.1 0.0 copy-done.2
  67.1 27.4 %output_scatter.1 = bf16[256,2048]{1,0:T(8,128)(2,1)S(1)} custom-call(bf16[1024,256]{1,0:T(8,128)(2,1)S(1)} %get-tuple-element.29.dm_ref, bf16[1024,256]{1,0:T(8,128)(2,1)S(1)} %get-tuple-element.30.cm_ref, bf16[256,2048]{1,0:T(8,128)(2,1)S(1)} %copy-done.1, bf16[256,2048]{1,0:T(8,128)(2,1)S(1)} %copy-done.2), custom_call_target="tpu_custom_call" | custom-call | flops 10000000000 | bytes 20000000 | tf_op jit(solution)/shard_map/output_scatter/pallas_call | solution.py:644
  94.5 1.0 %copy.23 = bf16[256,2048]{1,0:T(8,128)(2,1)} copy(bf16[256,2048]{1,0:T(8,128)(2,1)S(1)} %output_scatter.1) | data formatting | bytes 2097152
  (8 shorter events, 0.0 us)
Async XLA Ops:
  1.1 1.2 %copy-start = (bf16[1024,512]{1,0:T(8,128)(2,1)S(1)}, bf16[1024,512]{1,0:T(8,128)(2,1)}, u32[]{:S(2)}) copy-start(bf16[1024,512]{1,0:T(8,128)(2,1)} %refs_0_.1) | copy-start | bytes 3145732
  1.5 0.7 copy-start.7
  32.0 8.6 %copy-start.6 = (bf16[31,256]{1,0:T(8,128)(2,1)S(1)}, bf16[31,256]{1,0:T(8,128)(2,1)}, u32[]{:S(2)}) copy-start(bf16[31,256]{1,0:T(8,128)(2,1)} %param.29) | copy-start | bytes 47620
  32.0 8.6 %copy-start.4 = (f32[256]{0:T(256)S(1)}, f32[256]{0:T(256)}, u32[]{:S(2)}) copy-start(f32[256]{0:T(256)} %param.31) | copy-start | bytes 3076
  40.6 0.7 copy-start.3
  40.6 0.7 copy-start.5
  41.3 25.7 %copy-start.1 = (bf16[256,2048]{1,0:T(8,128)(2,1)S(1)}, bf16[256,2048]{1,0:T(8,128)(2,1)}, u32[]{:S(2)}) copy-start(bf16[256,2048]{1,0:T(8,128)(2,1)} %wd_ref.1) | copy-start | bytes 3145732
  41.3 25.8 %copy-start.2 = (bf16[256,2048]{1,0:T(8,128)(2,1)S(1)}, bf16[256,2048]{1,0:T(8,128)(2,1)}, u32[]{:S(2)}) copy-start(bf16[256,2048]{1,0:T(8,128)(2,1)} %wc_ref.1) | copy-start | bytes 3145732
where the time goes:
time: 95.7 us; the launch traced here: 95.5 us
  Pallas kernels  91.3 us (95%)
  local copies, waits for them, and re-layouts  3.56 us (4%)
    pallas_call x1, Pallas kernels, project(): pl.pallas_call(functools.partial(project_kernel, heads), out_shape=tuple(...  29.6 us
    pallas_call x1, Pallas kernels, output_projection(): pl.pallas_call(output_kernel, out_shape=jax.ShapeDtypeStruct((rows, width...  27.4 us
    pallas_call x1, Pallas kernels, middle(): pl.pallas_call(functools.partial(middle_kernel, heads, width), out_shape=...  25.7 us
    pallas_call x1, Pallas kernels, delta_rule(): pl.pallas_call(functools.partial(delta_kernel, heads, width), out_shape=(...  8.57 us
    unnamed x19, local copies, waits for them, and re-layouts  2.61 us

commit v1 on v0

--- a/solution.py
+++ b/solution.py
@@ -309,8 +309,8 @@
 def middle_kernel(
     heads, width, final_ref, gv_ref, gg_ref, cg_ref, taps_ref, ln_gain_ref, ln_shift_ref,
     outa_ref, outb_ref, dg_ref, gain_ref, mixed_ref, conv_ref,
-    padded, filtered, halo_out, halo_in, sums_out, sums_in, near, window_s, sent_s, far_s,
-    near_send, near_recv, far_send, far_recv, halo_send, halo_recv, ln_send, ln_recv,
+    padded, filtered, halo_out, halo_in, sums_out, sums_in, window_s, sent_s, far_s,
+    far_send, far_recv, halo_send, halo_recv, ln_send, ln_recv,
 ):
     rows = gv_ref.shape[0]
     halo = halo_in.shape[0]
@@ -320,21 +320,33 @@
     tiles = rows // BLOCK
     sp, place = lax.axis_size("sp"), lax.axis_index("sp")
     tp, me = lax.axis_size("tp"), lax.axis_index("tp")
-    reaches = [2]
+    reaches = [1]
     while 2 * reaches[-1] < sp:
         reaches.append(2 * reaches[-1])
-    distances = [1, 2] + reaches[1:]
+    last = len(reaches) - 1
     barrier = pltpu.get_barrier_semaphore()
-    for step in distances:
-        for to in (step, sp - step):
+    expected = tp - 1
+    for step in reaches:
+        ahead, behind = place + step < sp, place >= step
+
+        @pl.when(ahead)
+        def _(step=step):
             pl.semaphore_signal(
-                barrier, inc=1, device_id={"sp": lax.rem(place + to, sp)}, device_id_type=MESH
+                barrier, inc=1, device_id={"sp": place + step}, device_id_type=MESH
             )
+
+        @pl.when(behind)
+        def _(step=step):
+            pl.semaphore_signal(
+                barrier, inc=1, device_id={"sp": place - step}, device_id_type=MESH
+            )
+
+        expected = expected + ahead.astype(jnp.int32) + behind.astype(jnp.int32)
     for step in range(1, tp):
         pl.semaphore_signal(
             barrier, inc=1, device_id={"tp": lax.rem(me + step, tp)}, device_id_type=MESH
         )
-    pl.semaphore_wait(barrier, 2 * len(distances) + tp - 1)
+    pl.semaphore_wait(barrier, expected)
 
     def onward(src, dst, send, recv, step):
         return pltpu.make_async_remote_copy(
@@ -342,15 +354,52 @@
             dst_ref=dst,
             send_sem=send,
             recv_sem=recv,
-            device_id={"sp": lax.rem(place + step, sp)},
+            device_id={"sp": jnp.minimum(place + step, sp - 1)},
             device_id_type=MESH,
         )
 
-    firsts = [
-        onward(final_ref, near.at[i], near_send.at[i], near_recv.at[i], i + 1) for i in range(2)
-    ]
-    for copy in firsts:
-        copy.start()
+    def carry_copy(i, h):
+        cut = slice(width, 2 * width) if i == last else slice(0, 2 * width)
+        source = final_ref if i == 0 else sent_s.at[i - 1]
+        return onward(
+            source.at[h, :, cut], far_s.at[i, h, :, cut],
+            far_send.at[i, h], far_recv.at[i, h], reaches[i],
+        )
+
+    def send_carry(i, h):
+        @pl.when(place + reaches[i] < sp)
+        def _():
+            carry_copy(i, h).start()
+
+    def take_carry(i, h):
+        @pl.when(place >= reaches[i])
+        def _():
+            carry_copy(i, h).wait_recv()
+
+        @pl.when(place < reaches[i])
+        def _():
+            far_s[i, h] = jnp.zeros((width, 2 * width), jnp.bfloat16)
+
+    def combine(later, earlier):
+        moved = mm(later[:, :width], earlier)
+        return jnp.concatenate(
+            [moved[:, :width], moved[:, width:] + later[:, width:].astype(jnp.float32)], axis=1
+        )
+
+    def exchange(i):
+        for h in range(heads):
+            take_carry(i, h)
+            own = final_ref[h] if i == 0 else sent_s[i - 1, h]
+            sent_s[i, h] = combine(own, far_s[i, h]).astype(jnp.bfloat16)
+            send_carry(i + 1, h)
+        for h in range(heads):
+            if i == 0:
+                window_s[h] = far_s[i, h].astype(jnp.float32)
+            else:
+                window_s[h] = combine(window_s[h], far_s[i, h])
+
+    for h in range(heads):
+        send_carry(0, h)
 
     def at(t):
         return pl.ds(pl.multiple_of(t * BLOCK, BLOCK), BLOCK)
@@ -368,7 +417,10 @@
     units = unit(tiles - 1, 0)
     halo_out[...] = units[BLOCK - halo :, :]
     halo_copy = onward(halo_out, halo_in, halo_send.at[0], halo_recv.at[0], 1)
-    halo_copy.start()
+
+    @pl.when(place + 1 < sp)
+    def _():
+        halo_copy.start()
 
     def unit_loop(t, carry):
         unit(t, 0)
@@ -394,24 +446,19 @@
 
     half = tiles // 2
     lax.fori_loop(1, half, conv, 0)
-    for copy in firsts:
-        copy.wait()
-    for h in range(heads):
-        one = jnp.where(place >= 1, near[0, h].astype(jnp.float32), 0.0)
-        two = jnp.where(place >= 2, near[1, h].astype(jnp.float32), 0.0)
-        moved = mm(one[:, :width], two)
-        window_s[h] = jnp.concatenate(
-            [moved[:, :width], moved[:, width:] + one[:, width:]], axis=1
-        )
-        sent_s[0, h] = window_s[h].astype(jnp.bfloat16)
-
-    def step_copy(i):
-        return onward(sent_s.at[i], far_s.at[i], far_send.at[i], far_recv.at[i], reaches[i])
-
-    step_copy(0).start()
+    if last > 0:
+        exchange(0)
     lax.fori_loop(half, tiles, conv, 0)
-    halo_copy.wait()
-    before = jnp.where(place >= 1, halo_in[...].astype(jnp.float32), 0.0)
+
+    @pl.when(place >= 1)
+    def _():
+        halo_copy.wait_recv()
+
+    @pl.when(place < 1)
+    def _():
+        halo_in[...] = jnp.zeros(halo_in.shape, jnp.bfloat16)
+
+    before = halo_in[...].astype(jnp.float32)
     for g in range(groups):
         padded[g, :halo, :] = before[:, g * lanes : (g + 1) * lanes]
     conv(0, 0)
@@ -428,17 +475,8 @@
 
     for step in range(1, tp):
         ln_copy(step).start()
-    for i in range(len(reaches) - 1):
-        step_copy(i).wait()
-        for h in range(heads):
-            earlier = jnp.where(place >= reaches[i], far_s[i, h].astype(jnp.float32), 0.0)
-            window = window_s[h]
-            moved = mm(window[:, :width], earlier)
-            window_s[h] = jnp.concatenate(
-                [moved[:, :width], moved[:, width:] + window[:, width:]], axis=1
-            )
-            sent_s[i + 1, h] = window_s[h].astype(jnp.bfloat16)
-        step_copy(i + 1).start()
+    for i in range(1, last):
+        exchange(i)
     for step in range(1, tp):
         ln_copy(step).wait()
     channels = groups * lanes * tp
@@ -460,15 +498,14 @@
         return carry
 
     lax.fori_loop(0, tiles, norm, 0)
-    last = len(reaches) - 1
-    step_copy(last).wait()
     carried = []
     for h in range(heads):
-        earlier = jnp.where(
-            place >= reaches[last], far_s[last, h, :, width:].astype(jnp.float32), 0.0
-        )
-        window = window_s[h]
-        carried.append((mm(window[:, :width], earlier) + window[:, width:]).astype(jnp.bfloat16))
+        take_carry(last, h)
+        earlier = far_s[last, h, :, width:]
+        if last > 0:
+            window = window_s[h]
+            earlier = mm(window[:, :width], earlier) + window[:, width:]
+        carried.append(earlier.astype(jnp.bfloat16))
 
     def one_tile(t, carry):
         for h in range(heads):
@@ -484,6 +521,15 @@
         return carry
 
     lax.fori_loop(0, tiles, one_tile, 0)
+    for i in range(last + 1):
+        @pl.when(place + reaches[i] < sp)
+        def _(i=i):
+            for h in range(heads):
+                carry_copy(i, h).wait_send()
+
+    @pl.when(place + 1 < sp)
+    def _():
+        halo_copy.wait_send()
 
 
 def middle(final, glu_value, glu_gate, conv_gate, taps, ln_gain, ln_shift, outa, outb, gate, gain):
@@ -495,7 +541,7 @@
     groups = channels // lanes
     sp, tp = lax.axis_size("sp"), lax.axis_size("tp")
     steps = 1
-    while 2 ** (steps + 1) < sp:
+    while 2**steps < sp:
         steps += 1
     vm = pl.BlockSpec(memory_space=pltpu.VMEM)
     dma = pltpu.SemaphoreType.DMA
@@ -516,14 +562,11 @@
             pltpu.VMEM((halo, channels), jnp.bfloat16),
             pltpu.VMEM((tiles, 8, BLOCK), jnp.float32),
             pltpu.VMEM((tp - 1, tiles, 8, BLOCK), jnp.float32),
-            pltpu.VMEM((2,) + pair, jnp.bfloat16),
             pltpu.VMEM(pair, jnp.float32),
             pltpu.VMEM((steps,) + pair, jnp.bfloat16),
             pltpu.VMEM((steps,) + pair, jnp.bfloat16),
-            dma((2,)),
-            dma((2,)),
-            dma((steps,)),
-            dma((steps,)),
+            dma((steps, heads)),
+            dma((steps, heads)),
             dma((1,)),
             dma((1,)),
             dma((tp - 1,)),

time: 95.7 us -> 88 us (0.920)
  the two profiles are of different devices: /device:TPU:7 before, /device:TPU:9 now
where the time goes in v1:
time: 88 us; the launch traced here: 87.8 us
  Pallas kernels  83.7 us (95%)
  local copies, waits for them, and re-layouts  3.56 us (4%)
    pallas_call x1, Pallas kernels, project(): pl.pallas_call(functools.partial(project_kernel, heads), out_shape=tuple(...  29.6 us
    pallas_call x1, Pallas kernels, output_projection(): pl.pallas_call(output_kernel, out_shape=jax.ShapeDtypeStruct((rows, width...  27.4 us
    pallas_call x1, Pallas kernels, middle(): pl.pallas_call(functools.partial(middle_kernel, heads, width), out_shape=...  18.1 us
    pallas_call x1, Pallas kernels, delta_rule(): pl.pallas_call(functools.partial(delta_kernel, heads, width), out_shape=(...  8.57 us
    unnamed x19, local copies, waits for them, and re-layouts  2.61 us

profile of v1, /device:TPU:9, one launch (start us, length us, event | category | flops | bytes accessed | tf_op | source)
XLA Modules:
  0.0 87.8 jit_solution(2764197540597764178)
XLA Ops:
  0.0 0.8 constant_dynamic-slice_fusion
  0.8 0.3 copy.20
  1.1 0.0 copy-start
  1.1 0.3 copy.21
  1.4 0.1 pad.5.clone
  1.5 0.3 maximum_maximum_fusion.refs_8_
  1.9 0.3 copy-done.7
  2.2 0.1 dynamic-slice_exponential_fusion
  2.3 0.1 maximum_bitcast_fusion.refs_9_
  2.3 0.0 copy-done
  2.3 29.6 %gather_project.1 = (bf16[1024,256]{1,0:T(8,128)(2,1)S(1)}, bf16[1024,256]{1,0:T(8,128)(2,1)S(1)}, bf16[1024,256]{1,0:T(8,128)(2,1)S(1)}, bf16[1024,256]{1,0:T(8...) custom-call(bf16[1024,512]{1,0:T(8,128)(2,1)S(1)} %copy-done, ...), custom_call_target="tpu_custom_call" | custom-call | flops 10000000000 | bytes 20000000 | tf_op jit(solution)/shard_map/gather_project/pallas_call | solution.py:280
  32.0 0.0 copy-start.6
  32.0 0.0 copy-start.4
  32.0 8.6 %delta_rule.1 = (bf16[2,1024,128]{2,1,0:T(8,128)(2,1)S(1)}, f32[2,1024,128]{2,1,0:T(8,128)S(1)}, bf16[2,128,256]{2,1,0:T(8,128)(2,1)S(1)}) custom-call(bf16[1024,256]{1,0:T(8,128)(2,1)S(1)} %get-tuple-element.18.q_ref, bf16[1024,256]{1,0:T(8,128)(2,1)S(1)} %get-tuple-element.19.k_ref, bf16[1024,256]{1,0:T(8,128)(2,1)S(1)} %get-tuple-element.20.v_ref, ...), custom_call_target="tpu_custom_call" | custom-call | flops 10000000000 | bytes 4000000 | tf_op jit(solution)/shard_map/delta_rule/pallas_call | solution.py:128
  40.6 0.0 copy-done.6
  40.6 0.0 copy-start.3
  40.6 0.0 copy-start.5
  40.6 0.0 copy-done.4
  40.7 0.6 copy-done.3
  41.3 0.0 copy-done.5
  41.3 18.1 %exchange_middle.1 = (bf16[1024,256]{1,0:T(8,128)(2,1)S(1)}, bf16[1024,256]{1,0:T(8,128)(2,1)S(1)}) custom-call(bf16[2,128,256]{2,1,0:T(8,128)(2,1)S(1)} %get-tuple-element.22.final_ref, bf16[1024,256]{1,0:T(8,128)(2,1)S(1)} %get-tuple-element.23.gv_ref, bf16[1024,256]{1,0:T(8,128)(2,1)S(1)} %get-tuple-element.24.gg_ref, ...), custom_call_target="tpu_custom_call" | custom-call | flops 10000000000 | bytes 20000000 | tf_op jit(solution)/shard_map/exchange_middle/pallas_call | solution.py:550
  59.4 0.0 copy-done.1
  59.4 27.4 %output_scatter.1 = bf16[256,2048]{1,0:T(8,128)(2,1)S(1)} custom-call(bf16[1024,256]{1,0:T(8,128)(2,1)S(1)} %get-tuple-element.29.dm_ref, bf16[1024,256]{1,0:T(8,128)(2,1)S(1)} %get-tuple-element.30.cm_ref, bf16[256,2048]{1,0:T(8,128)(2,1)S(1)} %copy-done.1, bf16[256,2048]{1,0:T(8,128)(2,1)S(1)} %copy-done.2), custom_call_target="tpu_custom_call" | custom-call | flops 10000000000 | bytes 20000000 | tf_op jit(solution)/shard_map/output_scatter/pallas_call | solution.py:687
  86.8 1.0 %copy.23 = bf16[256,2048]{1,0:T(8,128)(2,1)} copy(bf16[256,2048]{1,0:T(8,128)(2,1)S(1)} %output_scatter.1) | data formatting | bytes 2097152
  (8 shorter events, 0.0 us)
Async XLA Ops:
  1.1 1.2 %copy-start = (bf16[1024,512]{1,0:T(8,128)(2,1)S(1)}, bf16[1024,512]{1,0:T(8,128)(2,1)}, u32[]{:S(2)}) copy-start(bf16[1024,512]{1,0:T(8,128)(2,1)} %refs_0_.1) | copy-start | bytes 3145732
  1.5 0.7 copy-start.7
  32.0 8.6 %copy-start.6 = (bf16[31,256]{1,0:T(8,128)(2,1)S(1)}, bf16[31,256]{1,0:T(8,128)(2,1)}, u32[]{:S(2)}) copy-start(bf16[31,256]{1,0:T(8,128)(2,1)} %param.29) | copy-start | bytes 47620
  32.0 8.6 %copy-start.4 = (f32[256]{0:T(256)S(1)}, f32[256]{0:T(256)}, u32[]{:S(2)}) copy-start(f32[256]{0:T(256)} %param.31) | copy-start | bytes 3076
  40.6 0.7 copy-start.3
  40.6 0.7 copy-start.5
  41.3 18.1 %copy-start.1 = (bf16[256,2048]{1,0:T(8,128)(2,1)S(1)}, bf16[256,2048]{1,0:T(8,128)(2,1)}, u32[]{:S(2)}) copy-start(bf16[256,2048]{1,0:T(8,128)(2,1)} %wd_ref.1) | copy-start | bytes 3145732
  41.3 18.1 %copy-start.2 = (bf16[256,2048]{1,0:T(8,128)(2,1)S(1)}, bf16[256,2048]{1,0:T(8,128)(2,1)}, u32[]{:S(2)}) copy-start(bf16[256,2048]{1,0:T(8,128)(2,1)} %wc_ref.1) | copy-start | bytes 3145732

commit v2 on v0

v2 whole, which is shorter than its diff:
```python
import functools

import jax
import jax.numpy as jnp
from jax import lax
from jax.experimental import pallas as pl
from jax.experimental.pallas import tpu as pltpu
from jax.sharding import PartitionSpec as P

BLOCK = 128
PROJECTIONS = 7
QUERY, KEY, VALUE, DELTA_GATE, GLU_VALUE, GLU_GATE, CONV_GATE = range(PROJECTIONS)
OUT_CUT = 512
TINY_NORM = 1e-06
TINY_VAR = 1e-05
HIGHEST = lax.Precision.HIGHEST
MESH = pl.DeviceIdType.MESH


def nt(a, b):
    return lax.dot_general(a, b, (((1,), (1,)), ((), ())), preferred_element_type=jnp.float32)


def mm(a, b):
    return jnp.dot(
        a.astype(jnp.bfloat16), b.astype(jnp.bfloat16), preferred_element_type=jnp.float32
    )


def slice_shape(rows, columns, pieces):
    high = max(16, rows // pieces)
    across = pieces // (rows // high)
    return high, columns // across, across


def layer_kernel(
    heads, width,
    tok_hbm, wq_hbm, wk_hbm, wv_hbm, wdg_hbm, wgv_hbm, wgg_hbm, wcg_hbm,
    beta_hbm, decay_hbm, rate_hbm, gain_hbm, taps_hbm, ln_gain_hbm, ln_shift_hbm,
    out_delta_hbm, out_conv_hbm,
    out_ref,
    full, w_s, beta_s, decay_s, rate_s, gain_ref, taps_s, ln_gain_ref, ln_shift_ref,
    wg_s, rate_row, taps_ref, proj, gates_s, wfull,
    lhs_s, corr_s, score_s, wt_s, tail_s, state_ref, outa_ref, outb_ref, final_ref,
    padded, filtered, halo_out, halo_in, sums_out, sums_in, window_s, sent_s, far_s,
    mixed_out, mixed_in, acc_s,
    tok_sem, w_sem, small_sem, ow_sem,
    y_send, y_recv, own_send, own_recv, fwd_send, fwd_recv,
    wo_send, wo_recv, wy_send, wy_recv, wl_send, wl_recv, wx_send, wx_recv, wb_send, wb_recv,
    far_send, far_recv, halo_send, halo_recv, ln_send, ln_recv, mix_send, mix_recv,
):
    rows = full.shape[0]
    tp, me = lax.axis_size("tp"), lax.axis_index("tp")
    sp, place = lax.axis_size("sp"), lax.axis_index("sp")
    part = full.shape[1] // tp
    chips = tp // 2
    core = lax.rem(me, 2)
    chip = me // 2
    sibling = me + 1 - 2 * core
    tiles = rows // BLOCK
    halo = halo_in.shape[0]
    lanes = padded.shape[2]
    groups = padded.shape[0]
    kernel = taps_s.shape[0]
    line = sp // 2
    spot = place // 2
    side = lax.rem(place, 2)

    def at(t, count=1):
        return pl.ds(pl.multiple_of(t * BLOCK, BLOCK), count * BLOCK)

    def columns(owner):
        return pl.ds(pl.multiple_of(owner * part, part), part)

    token_loads = [
        pltpu.make_async_copy(
            tok_hbm.at[at(r), :], full.at[at(r), columns(me)], tok_sem.at[r]
        )
        for r in range(tiles)
    ]
    out_loads = [
        pltpu.make_async_copy(src, wfull.at[i, me], ow_sem.at[i])
        for i, src in enumerate((out_delta_hbm, out_conv_hbm))
    ]
    w_loads = [
        pltpu.make_async_copy(src, w_s.at[i], w_sem.at[i])
        for i, src in enumerate((wq_hbm, wk_hbm, wv_hbm, wdg_hbm, wgv_hbm, wgg_hbm, wcg_hbm))
    ]
    small_loads = [
        pltpu.make_async_copy(src, dst, small_sem.at[i])
        for i, (src, dst) in enumerate((
            (beta_hbm, beta_s), (decay_hbm, decay_s), (rate_hbm, rate_s), (gain_hbm, gain_ref),
            (taps_hbm, taps_s), (ln_gain_hbm, ln_gain_ref), (ln_shift_hbm, ln_shift_ref),
        ))
    ]
    token_loads[0].start()
    for load in out_loads + token_loads[1:] + small_loads + w_loads:
        load.start()

    reaches = [1]
    while 2 * reaches[-1] < sp:
        reaches.append(2 * reaches[-1])
    last = len(reaches) - 1
    distances = sorted(set(reaches) | set(range(2, sp, 2)))
    barrier = pltpu.get_barrier_semaphore()
    expected = tp - 1
    for step in range(1, tp):
        pl.semaphore_signal(
            barrier, inc=1, device_id={"tp": lax.rem(me + step, tp)}, device_id_type=MESH
        )
    for step in distances:
        ahead, behind = place + step < sp, place >= step

        @pl.when(ahead)
        def _(step=step):
            pl.semaphore_signal(
                barrier, inc=1, device_id={"sp": place + step}, device_id_type=MESH
            )

        @pl.when(behind)
        def _(step=step):
            pl.semaphore_signal(
                barrier, inc=1, device_id={"sp": place - step}, device_id_type=MESH
            )

        expected = expected + ahead.astype(jnp.int32) + behind.astype(jnp.int32)
    pl.semaphore_wait(barrier, expected)

    def to_tp(src, dst, send, recv, there):
        return pltpu.make_async_remote_copy(
            src_ref=src, dst_ref=dst, send_sem=send, recv_sem=recv,
            device_id={"tp": there}, device_id_type=MESH,
        )

    def to_sp(src, dst, send, recv, there):
        return pltpu.make_async_remote_copy(
            src_ref=src, dst_ref=dst, send_sem=send, recv_sem=recv,
            device_id={"sp": there}, device_id_type=MESH,
        )

    def far_peer(o):
        return lax.rem(chip + o, chips) * 2 + core

    def far_owner(o):
        return lax.rem(chip - o + chips, chips) * 2 + core

    def across(o, r):
        block = full.at[at(r), columns(me)]
        return to_tp(block, block, y_send.at[o - 1, r], y_recv.at[o - 1, r], far_peer(o))

    def beside(r):
        block = full.at[at(r), columns(me)]
        return to_tp(block, block, own_send.at[r], own_recv.at[r], sibling)

    def forward(o, r):
        block = full.at[at(r), columns(far_owner(o))]
        return to_tp(block, block, fwd_send.at[o - 1, r], fwd_recv.at[o - 1, r], sibling)

    high, broad, split = slice_shape(wfull.shape[2], wfull.shape[3], sp)

    def weight_slice(owner, index):
        top = pl.ds(pl.multiple_of(index // split * high, high), high)
        left = pl.ds(pl.multiple_of(lax.rem(index, split) * broad, broad), broad)
        return wfull.at[:, owner, top, left]

    def weights_beside():
        return to_tp(wfull.at[:, me], wfull.at[:, me], wo_send.at[0], wo_recv.at[0], sibling)

    def weights_across(o):
        piece = weight_slice(me, place)
        return to_tp(piece, piece, wy_send.at[o - 1], wy_recv.at[o - 1], far_peer(o))

    def weights_along(o, there, origin):
        piece = weight_slice(far_owner(o), 2 * origin + side)
        return to_sp(
            piece, piece, wl_send.at[o - 1, there], wl_recv.at[o - 1, origin], 2 * there + side
        )

    def weights_pair(o, j, parity):
        piece = weight_slice(far_owner(o), 2 * j + parity)
        return to_sp(
            piece, piece, wx_send.at[o - 1, j], wx_recv.at[o - 1, j], place + 1 - 2 * side
        )

    def weights_forward(o):
        block = wfull.at[:, far_owner(o)]
        return to_tp(block, block, wb_send.at[o - 1], wb_recv.at[o - 1], sibling)

    def both_ways(step, action):
        for there, valid in ((spot + step, spot + step < line), (spot - step, spot >= step)):
            @pl.when(valid)
            def _(there=there):
                action(jnp.clip(there, 0, line - 1))

    def spread_weights():
        for o in range(1, chips):
            weights_across(o).wait_recv()
        for step in range(1, line):
            def send(there):
                for o in range(1, chips):
                    weights_along(o, there, spot).start()

            both_ways(step, send)
        for o in range(1, chips):
            weights_pair(o, spot, side).start()

    def relay_weights(step):
        def relay(origin):
            for o in range(1, chips):
                weights_along(o, origin, origin).wait_recv()
                weights_pair(o, origin, side).start()

        both_ways(step, relay)

    def collect_weights():
        for o in range(1, chips):
            for j in range(line):
                weights_pair(o, j, 1 - side).wait_recv()
            weights_forward(o).start()

    for load in out_loads:
        load.wait()
    for o in range(1, chips):
        weights_across(o).start()
    for r in range(tiles):
        token_loads[r].wait()
        for o in range(1, chips):
            across(o, r).start()
        beside(r).start()
    weights_beside().start()
    for load in small_loads:
        load.wait()

    first_head = me * heads
    total_heads = beta_s.shape[0]
    lane_row = lax.broadcasted_iota(jnp.int32, (1, BLOCK), 1)
    rate = jnp.zeros((1, BLOCK), jnp.float32)
    for h in range(total_heads):
        value = jnp.exp(jnp.broadcast_to(rate_s[:, h : h + 1], (1, BLOCK)))
        rate = jnp.where(lane_row == h - first_head + heads, value, rate)
    rate = jnp.where((lane_row >= heads) & (lane_row < 2 * heads), rate, 0.0)
    rate_row[...] = rate
    pick_row = lax.broadcasted_iota(jnp.int32, (BLOCK, total_heads), 0)
    pick_col = lax.broadcasted_iota(jnp.int32, (BLOCK, total_heads), 1)
    pick_beta = (pick_row < heads) & (pick_col == pick_row + first_head)
    pick_decay = (
        (pick_row >= heads) & (pick_row < 2 * heads) & (pick_col == pick_row - heads + first_head)
    )
    wg_s[...] = (
        mm(jnp.where(pick_beta, 1.0, 0.0), beta_s[...])
        + mm(jnp.where(pick_decay, 1.0, 0.0), decay_s[...])
    ).astype(jnp.bfloat16)
    taps_ref[...] = taps_s[...].astype(jnp.float32)

    def receive(first, count):
        for i in range(count):
            for o in range(1, chips):
                across(o, first + i).wait_recv()
                forward(o, first + i).start()
        for i in range(count):
            beside(first + i).wait_recv()
            for o in range(1, chips):
                forward(o, first + i).wait_recv()

    def project(first, count):
        size = count * BLOCK
        here = at(first, count)
        squares = jnp.zeros((size, 1), jnp.float32)
        for b in range(tp):
            piece = full[here, b * part : (b + 1) * part].astype(jnp.float32)
            squares = squares + jnp.sum(piece * piece, axis=1, keepdims=True)
        inv_rms = lax.rsqrt(squares / (part * tp) + TINY_NORM)
        raw = nt(full[here, :], wg_s[...]) * inv_rms
        lane = lax.broadcasted_iota(jnp.int32, raw.shape, 1)
        softplus = jnp.maximum(raw, 0.0) + jnp.log1p(jnp.exp(-jnp.abs(raw)))
        gates_s[here, :] = jnp.where(
            lane < heads, jax.nn.sigmoid(raw), -rate_row[...] * softplus
        )
        for i in range(PROJECTIONS):
            summed = jnp.dot(full[here, :], w_s[i], preferred_element_type=jnp.float32)
            proj[i, here, :] = (summed * inv_rms).astype(jnp.bfloat16)

    row_id = lax.broadcasted_iota(jnp.int32, (BLOCK, BLOCK), 0)
    col_id = lax.broadcasted_iota(jnp.int32, (BLOCK, BLOCK), 1)
    causal = row_id >= col_id
    strict = row_id > col_id
    differ = row_id ^ col_id
    eye = jnp.where(row_id == col_id, 1.0, 0.0)
    tril = jnp.where(causal, 1.0, 0.0)

    def prepare(c):
        here = at(c)
        gates = gates_s[here, :]
        sums = jnp.dot(tril, gates, precision=HIGHEST, preferred_element_type=jnp.float32)
        chains = []
        for h in range(heads):
            cut = slice(h * width, (h + 1) * width)
            k, q = proj[KEY, here, cut], proj[QUERY, here, cut]
            v = proj[VALUE, here, cut].astype(jnp.float32)
            kf, qf = k.astype(jnp.float32), q.astype(jnp.float32)
            ik = lax.rsqrt(jnp.sum(kf * kf, axis=-1, keepdims=True) + TINY_NORM)
            iq = lax.rsqrt(jnp.sum(qf * qf, axis=-1, keepdims=True) + TINY_NORM)
            iq = iq * width ** (-0.5)
            beta = gates[:, h : h + 1]
            log_sum = sums[:, heads + h : heads + h + 1]
            log_full = jnp.broadcast_to(log_sum, (BLOCK, BLOCK))
            spread = log_full - log_full.T
            damp = jnp.where(causal, jnp.exp(jnp.where(causal, spread, 0.0)), 0.0)
            damp = damp * jnp.broadcast_to(ik, (BLOCK, BLOCK)).T
            lower = jnp.where(strict, nt(k, k) * damp * (beta * ik), 0.0)
            score_s[h, here, :] = (nt(q, k) * damp * iq).astype(jnp.bfloat16)
            grow = jnp.exp(log_sum)
            right = jnp.concatenate([v * beta, kf * (beta * ik * grow)], axis=1)
            tail = log_full[BLOCK - 1 : BLOCK, :]
            weighted = kf * (ik * jnp.exp(tail[:, :1] - log_sum))
            wt_s[h, c] = weighted.T.astype(jnp.bfloat16)
            tail_s[h, c] = jnp.broadcast_to(jnp.exp(tail), (8, BLOCK))
            lhs_s[h, c, BLOCK:, :] = (qf * (iq * grow)).astype(jnp.bfloat16)
            chains.append([h, lower, right, eye - jnp.where(differ == 1, lower, 0.0)])
        return here, c, chains

    def blocks(first, count):
        prepared = [prepare(first + i) for i in range(count)]
        size = 2
        while size < BLOCK:
            level = (differ >= size) & (differ < 2 * size)
            parts = [
                [mm(jnp.where(level, ch[1], 0.0), ch[3]) for ch in item[2]] for item in prepared
            ]
            for item, moves in zip(prepared, parts):
                for ch, moved in zip(item[2], moves):
                    ch[3] = ch[3] - mm(ch[3], moved)
            size *= 2
        for here, c, chains in prepared:
            for h, lower, right, inverse in chains:
                solved = mm(inverse, right)
                corr_s[h, here, :] = solved[:, :width]
                lhs_s[h, c, :BLOCK, :] = solved[:, width:].astype(jnp.bfloat16)

    def advance(c):
        here = at(c)
        boths = [mm(lhs_s[h, c], state_ref[h]) for h in range(heads)]
        fresh = []
        for h in range(heads):
            first = boths[h][:BLOCK]
            fresh.append(
                jnp.concatenate(
                    [-first[:, :width], corr_s[h, here, :] - first[:, width:]], axis=1
                ).astype(jnp.bfloat16)
            )
        for h in range(heads):
            decay = tail_s[h, c][:1, :]
            decay = jnp.concatenate([decay, decay], axis=1)
            state_ref[h] = state_ref[h] * decay + mm(wt_s[h, c], fresh[h])
        for h in range(heads):
            out = boths[h][BLOCK:] + mm(score_s[h, here, :], fresh[h])
            outa_ref[h, here, :] = out[:, :width].astype(jnp.bfloat16)
            outb_ref[h, here, :] = out[:, width:]

    def unit(t):
        value = proj[GLU_VALUE, at(t), :].astype(jnp.float32)
        gate = proj[GLU_GATE, at(t), :].astype(jnp.float32)
        units = (value * jax.nn.sigmoid(gate)).astype(jnp.bfloat16)
        wide = units.astype(jnp.float32)
        for g in range(groups):
            padded[g, pl.ds(pl.multiple_of(t * BLOCK + halo, halo), BLOCK), :] = wide[
                :, g * lanes : (g + 1) * lanes
            ]
        return units

    def conv(t, carry=0):
        first = jnp.zeros((BLOCK, 1), jnp.float32)
        second = jnp.zeros((BLOCK, 1), jnp.float32)
        for g in range(groups):
            total = jnp.zeros((BLOCK, lanes), jnp.float32)
            for j in range(kernel):
                start = t * BLOCK + (halo - kernel + 1 + j)
                tap = taps_ref[j : j + 1, g * lanes : (g + 1) * lanes]
                total = total + padded[g, pl.ds(start, BLOCK), :] * tap
            filtered[g, at(t), :] = total
            first = first + jnp.sum(total, axis=1, keepdims=True)
            second = second + jnp.sum(total * total, axis=1, keepdims=True)
        lane = lax.broadcasted_iota(jnp.int32, (BLOCK, BLOCK), 1)
        sums_out[t] = jnp.where(lane == 0, first, jnp.where(lane == 1, second, 0.0)).T[:8, :]
        return carry

    for h in range(heads):
        state_ref[h] = jnp.concatenate([eye, jnp.zeros((width, width), jnp.float32)], axis=1)
    for load in w_loads:
        load.wait()
    spread_weights()
    receive(0, 2)
    project(0, 2)

    def pair(i, carry):
        receive(2 * i, 2)
        relay_weights(i)
        project(2 * i, 2)
        blocks(2 * i - 2, 2)
        for n in range(2):
            advance(2 * i - 2 + n)
            unit(2 * i - 2 + n)

        def filter_tile(t, inner):
            @pl.when(t > 0)
            def _():
                conv(t)

            return inner

        lax.fori_loop(2 * i - 2, 2 * i, filter_tile, 0)
        return carry

    paired = tiles // 2 - 1
    lax.fori_loop(1, paired, pair, 0)
    for step in range(paired, line):
        relay_weights(step)
    tail = 2 * paired
    receive(tail, 1)
    project(tail, 1)
    blocks(tail - 2, 2)
    for n in range(2):
        advance(tail - 2 + n)
    receive(tail + 1, 1)
    project(tail + 1, 1)
    units = unit(tail + 1)
    halo_out[...] = units[BLOCK - halo :, :]
    halo_copy = to_sp(
        halo_out, halo_in, halo_send.at[0], halo_recv.at[0], jnp.minimum(place + 1, sp - 1)
    )

    @pl.when(place + 1 < sp)
    def _():
        halo_copy.start()

    blocks(tail, 2)
    for n in range(2):
        advance(tail + n)
    final_ref[...] = state_ref[...].astype(jnp.bfloat16)

    def carry_copy(i, h):
        cut = slice(width, 2 * width) if i == last else slice(0, 2 * width)
        source = final_ref if i == 0 else sent_s.at[i - 1]
        return to_sp(
            source.at[h, :, cut], far_s.at[i, h, :, cut], far_send.at[i, h], far_recv.at[i, h],
            jnp.minimum(place + reaches[i], sp - 1),
        )

    def send_carry(i, h):
        @pl.when(place + reaches[i] < sp)
        def _():
            carry_copy(i, h).start()

    def take_carry(i, h):
        @pl.when(place >= reaches[i])
        def _():
            carry_copy(i, h).wait_recv()

        @pl.when(place < reaches[i])
        def _():
            far_s[i, h] = jnp.zeros((width, 2 * width), jnp.bfloat16)

    def combine(later, earlier):
        moved = mm(later[:, :width], earlier)
        return jnp.concatenate(
            [moved[:, :width], moved[:, width:] + later[:, width:].astype(jnp.float32)], axis=1
        )

    def exchange(i):
        for h in range(heads):
            take_carry(i, h)
            own = final_ref[h] if i == 0 else sent_s[i - 1, h]
            sent_s[i, h] = combine(own, far_s[i, h]).astype(jnp.bfloat16)
            send_carry(i + 1, h)
        for h in range(heads):
            if i == 0:
                window_s[h] = far_s[i, h].astype(jnp.float32)
            else:
                window_s[h] = combine(window_s[h], far_s[i, h])

    for h in range(heads):
        send_carry(0, h)

    for n in range(3):
        unit(tail - 2 + n)
    lax.fori_loop(tail - 2, tail + 2, conv, 0)

    @pl.when(place >= 1)
    def _():
        halo_copy.wait_recv()

    @pl.when(place < 1)
    def _():
        halo_in[...] = jnp.zeros(halo_in.shape, jnp.bfloat16)

    before = halo_in[...].astype(jnp.float32)
    for g in range(groups):
        padded[g, :halo, :] = before[:, g * lanes : (g + 1) * lanes]
    conv(0)

    def ln_copy(step):
        return to_tp(
            sums_out, sums_in.at[step - 1], ln_send.at[step - 1], ln_recv.at[step - 1],
            lax.rem(me + step, tp),
        )

    for step in range(1, tp):
        ln_copy(step).start()
    if last > 0:
        exchange(0)
    for step in range(1, tp):
        ln_copy(step).wait_recv()
    channels = groups * lanes * tp
    per = tiles // tp

    def mixed_copy(kind, there):
        return to_tp(
            mixed_out.at[kind, there], mixed_in.at[kind, me],
            mix_send.at[kind, there], mix_recv.at[kind, me], there,
        )

    def mixed_wait(kind, source):
        to_tp(
            mixed_out.at[kind, source], mixed_in.at[kind, source],
            mix_send.at[kind, source], mix_recv.at[kind, source], source,
        ).wait_recv()

    far_targets = [
        lax.rem(chip + o, chips) * 2 + lax.rem(core + c, 2) for o in range(1, chips) for c in (0, 1)
    ]

    def norm(target):
        def tile(i, carry):
            t = target * per + i
            here = pl.ds(pl.multiple_of(i * BLOCK, BLOCK), BLOCK)
            sums = sums_out[t]
            for step in range(1, tp):
                sums = sums + sums_in[step - 1, t]
            sums = jnp.concatenate([sums, jnp.zeros((BLOCK - 8, BLOCK), jnp.float32)], axis=0).T
            center = sums[:, 0:1] / channels
            variance = jnp.maximum(sums[:, 1:2] / channels - center * center, 0.0)
            scale = lax.rsqrt(variance + TINY_VAR)
            for g in range(groups):
                cut = slice(g * lanes, (g + 1) * lanes)
                normed = (filtered[g, at(t), :] - center) * scale
                normed = normed * ln_gain_ref[:, cut] + ln_shift_ref[:, cut]
                gate = proj[CONV_GATE, at(t), cut].astype(jnp.float32)
                mixed_out[1, target, here, cut] = (
                    jax.nn.silu(normed) * jax.nn.silu(gate)
                ).astype(jnp.bfloat16)
            return carry

        lax.fori_loop(0, per, tile, 0)

    for target in far_targets + [sibling]:
        norm(target)
        mixed_copy(1, target).start()
    norm(me)
    for i in range(1, last):
        exchange(i)
    collect_weights()

    def out_columns(n):
        return pl.ds(pl.multiple_of(n * OUT_CUT, OUT_CUT), OUT_CUT)

    cuts = out_ref.shape[1] // OUT_CUT
    sources = [sibling] + far_targets
    for source in sources:
        mixed_wait(1, source)
    weights_beside().wait_recv()
    for o in range(1, chips):
        weights_forward(o).wait_recv()

    def conv_part(n, carry):
        total = jnp.dot(
            mixed_out[1, me], wfull[1, me, :, out_columns(n)], preferred_element_type=jnp.float32
        )
        for source in sources:
            total = total + jnp.dot(
                mixed_in[1, source], wfull[1, source, :, out_columns(n)],
                preferred_element_type=jnp.float32,
            )
        acc_s[:, out_columns(n)] = total
        return carry

    lax.fori_loop(0, cuts, conv_part, 0)

    carried = []
    for h in range(heads):
        take_carry(last, h)
        earlier = far_s[last, h, :, width:]
        if last > 0:
            window = window_s[h]
            earlier = mm(window[:, :width], earlier) + window[:, width:]
        carried.append(earlier.astype(jnp.bfloat16))

    def attend(target):
        def tile(i, carry):
            t = target * per + i
            here = pl.ds(pl.multiple_of(i * BLOCK, BLOCK), BLOCK)
            for h in range(heads):
                cut = slice(h * width, (h + 1) * width)
                result = outb_ref[h, at(t), :] + mm(outa_ref[h, at(t), :], carried[h])
                result = result * lax.rsqrt(
                    jnp.mean(result * result, axis=-1, keepdims=True) + TINY_NORM
                )
                gate = proj[DELTA_GATE, at(t), cut].astype(jnp.float32)
                mixed_out[0, target, here, cut] = (
                    result * gain_ref[...] * jax.nn.silu(gate)
                ).astype(jnp.bfloat16)
            return carry

        lax.fori_loop(0, per, tile, 0)

    for target in far_targets + [sibling]:
        attend(target)
        mixed_copy(0, target).start()
    attend(me)
    mixed_wait(0, sibling)

    def near_part(n, carry):
        total = jnp.dot(
            mixed_out[0, me], wfull[0, me, :, out_columns(n)], preferred_element_type=jnp.float32
        )
        total = total + jnp.dot(
            mixed_in[0, sibling], wfull[0, sibling, :, out_columns(n)],
            preferred_element_type=jnp.float32,
        )
        acc_s[:, out_columns(n)] = acc_s[:, out_columns(n)] + total
        return carry

    lax.fori_loop(0, cuts, near_part, 0)
    for index, source in enumerate(far_targets):
        mixed_wait(0, source)

        def far_part(n, carry, source=source, closing=index + 1 == len(far_targets)):
            total = acc_s[:, out_columns(n)] + jnp.dot(
                mixed_in[0, source], wfull[0, source, :, out_columns(n)],
                preferred_element_type=jnp.float32,
            )
            if closing:
                out_ref[:, out_columns(n)] = total.astype(jnp.bfloat16)
            else:
                acc_s[:, out_columns(n)] = total
            return carry

        lax.fori_loop(0, cuts, far_part, 0)

    for r in range(tiles):
        for o in range(1, chips):
            across(o, r).wait_send()
            forward(o, r).wait_send()
        beside(r).wait_send()
    weights_beside().wait_send()
    for o in range(1, chips):
        weights_across(o).wait_send()
        weights_forward(o).wait_send()
        for j in range(line):
            weights_pair(o, j, side).wait_send()
    for step in range(1, line):
        def sent(there):
            for o in range(1, chips):
                weights_along(o, there, spot).wait_send()

        both_ways(step, sent)
    for i in range(last + 1):
        @pl.when(place + reaches[i] < sp)
        def _(i=i):
            for h in range(heads):
                carry_copy(i, h).wait_send()

    @pl.when(place + 1 < sp)
    def _():
        halo_copy.wait_send()

    for step in range(1, tp):
        ln_copy(step).wait_send()
    for kind in range(2):
        for target in sources:
            mixed_copy(kind, target).wait_send()


def layer(tokens, weights, w_beta, w_decay, decay_log, gain, taps, ln_gain, ln_shift, out_delta, out_conv):
    rows, part = tokens.shape
    width = gain.shape[1]
    features, held = weights[0].shape
    heads = held // width
    channels = taps.shape[1]
    depth, columns = out_delta.shape
    kernel = taps.shape[0]
    halo = (kernel - 1 + 31) // 32 * 32
    lanes = min(channels, 128)
    groups = channels // lanes
    sp, tp = lax.axis_size("sp"), lax.axis_size("tp")
    others = max(tp // 2 - 1, 1)
    line = sp // 2
    steps = 1
    while 2**steps < sp:
        steps += 1
    tiles = rows // BLOCK
    slot = rows // tp
    dma = pltpu.SemaphoreType.DMA
    pair = (heads, width, 2 * width)
    bf16, f32 = jnp.bfloat16, jnp.float32
    vmem = pltpu.VMEM
    return pl.pallas_call(
        functools.partial(layer_kernel, heads, width),
        out_shape=jax.ShapeDtypeStruct((slot, columns), bf16),
        in_specs=[pl.BlockSpec(memory_space=pl.ANY)] * 17,
        out_specs=pl.BlockSpec(memory_space=pltpu.VMEM),
        scratch_shapes=[
            vmem((rows, features), bf16),
            vmem((PROJECTIONS, features, held), bf16),
            vmem(w_beta.shape, bf16),
            vmem(w_decay.shape, bf16),
            vmem(decay_log.shape, f32),
            vmem(gain.shape, f32),
            vmem(taps.shape, bf16),
            vmem(ln_gain.shape, f32),
            vmem(ln_shift.shape, f32),
            vmem((BLOCK, features), bf16),
            vmem((1, BLOCK), f32),
            vmem(taps.shape, f32),
            vmem((PROJECTIONS, rows, held), bf16),
            vmem((rows, BLOCK), f32),
            vmem((2, tp, depth, columns), bf16),
            vmem((heads, tiles, 2 * BLOCK, width), bf16),
            vmem((heads, rows, width), f32),
            vmem((heads, rows, BLOCK), bf16),
            vmem((heads, tiles, width, BLOCK), bf16),
            vmem((heads, tiles, 8, BLOCK), f32),
            vmem(pair, f32),
            vmem((heads, rows, width), bf16),
            vmem((heads, rows, width), f32),
            vmem(pair, bf16),
            vmem((groups, halo + rows, lanes), f32),
            vmem((groups, rows, lanes), f32),
            vmem((halo, channels), bf16),
            vmem((halo, channels), bf16),
            vmem((tiles, 8, BLOCK), f32),
            vmem((tp - 1, tiles, 8, BLOCK), f32),
            vmem(pair, f32),
            vmem((steps,) + pair, bf16),
            vmem((steps,) + pair, bf16),
            vmem((2, tp, slot, channels), bf16),
            vmem((2, tp, slot, channels), bf16),
            vmem((slot, columns), f32),
            dma((tiles,)),
            dma((PROJECTIONS,)),
            dma((7,)),
            dma((2,)),
            dma((others, tiles)),
            dma((others, tiles)),
            dma((tiles,)),
            dma((tiles,)),
            dma((others, tiles)),
            dma((others, tiles)),
            dma((1,)),
            dma((1,)),
            dma((others,)),
            dma((others,)),
            dma((others, line)),
            dma((others, line)),
            dma((others, line)),
            dma((others, line)),
            dma((others,)),
            dma((others,)),
            dma((steps, heads)),
            dma((steps, heads)),
            dma((1,)),
            dma((1,)),
            dma((tp - 1,)),
            dma((tp - 1,)),
            dma((2, tp)),
            dma((2, tp)),
        ],
        compiler_params=pltpu.CompilerParams(
            collective_id=0, has_side_effects=True, vmem_limit_bytes=60 * 1024 * 1024
        ),
        cost_estimate=pl.CostEstimate(
            flops=20_000_000_000, bytes_accessed=20_000_000, transcendentals=0
        ),
        name="layer",
    )(
        tokens, *weights, w_beta, w_decay, decay_log, gain, taps, ln_gain, ln_shift,
        out_delta, out_conv,
    )


def local(
    tokens,
    w_query,
    w_key,
    w_value,
    w_delta_gate,
    w_glu_value,
    w_glu_gate,
    w_conv_gate,
    w_beta,
    w_decay,
    decay_log,
    head_gain,
    conv_taps,
    ln_gain,
    ln_shift,
    out_delta,
    out_conv,
):
    weights = (w_query, w_key, w_value, w_delta_gate, w_glu_value, w_glu_gate, w_conv_gate)
    return layer(
        tokens,
        weights,
        w_beta.T,
        w_decay.T,
        decay_log[None, :],
        head_gain[None, :],
        conv_taps,
        ln_gain[None, :],
        ln_shift[None, :],
        out_delta,
        out_conv,
    )


def solution(mesh):
    return jax.shard_map(
        local,
        mesh=mesh,
        in_specs=(
            P("sp", "tp"),
            P(None, "tp"),
            P(None, "tp"),
            P(None, "tp"),
            P(None, "tp"),
            P(None, "tp"),
            P(None, "tp"),
            P(None, "tp"),
            P(),
            P(),
            P(),
            P(),
            P(None, "tp"),
            P("tp"),
            P("tp"),
            P("tp", None),
            P("tp", None),
        ),
        out_specs=P(("sp", "tp"), None),
        check_vma=False,
    )
```

time: 95.7 us -> 85.8 us (0.90)
  the two profiles are of different devices: /device:TPU:7 before, /device:TPU:9 now
where the time goes in v2:
time: 85.8 us; the launch traced here: 85.1 us
  Pallas kernels  82.8 us (97%)
  local copies, waits for them, and re-layouts  2.3 us (3%)
    pallas_call x1, Pallas kernels, layer(): pl.pallas_call(functools.partial(layer_kernel, heads, width), out_shape=j...  82.8 us
    unnamed x1, local copies, waits for them, and re-layouts  2.3 us

profile of v2, /device:TPU:9, one launch (start us, length us, event | category | flops | bytes accessed | tf_op | source)
XLA Modules:
  0.0 85.1 jit_solution(4786719531481423912)
XLA Ops:
  0.0 82.8 %layer.1 = bf16[256,2048]{1,0:T(8,128)(2,1)} custom-call(bf16[1024,512]{1,0:T(8,128)(2,1)} %tok_hbm.1, bf16[2048,256]{1,0:T(8,128)(2,1)} %wq_hbm.1, bf16[2048,256]{1,0:T(8,128)(2,1)} %wk_hbm.1, bf16[2048,256]{1,0:T(8,128)(2,1)} %wv_hbm.1, bf16[2048,256]{1,0:T(8,128)(2,1)} %wdg_hbm.1, bf16[2048,256]{1,0:T(8,128)(2,1)} %wgv_hbm.1, bf16[2048,256]{1,0:T(8,128)(2,1)} %wgg_hbm.1, ...), custom_call_target="tpu_custom_call" | custom-call | flops 20000000000 | bytes 20000000 | tf_op jit(solution)/shard_map/layer/pallas_call | solution.py:706
  82.8 2.3 %copy.19 = bf16[256,2048]{1,0:T(8,128)(2,1)} copy(bf16[256,2048]{1,0:T(8,128)(2,1)} %layer.1) | data formatting | bytes 2097152

commit v3 on v2

--- a/solution.py
+++ b/solution.py
@@ -101,14 +101,13 @@
     while 2 * reaches[-1] < sp:
         reaches.append(2 * reaches[-1])
     last = len(reaches) - 1
-    distances = sorted(set(reaches) | set(range(2, sp, 2)))
     barrier = pltpu.get_barrier_semaphore()
     expected = tp - 1
     for step in range(1, tp):
         pl.semaphore_signal(
             barrier, inc=1, device_id={"tp": lax.rem(me + step, tp)}, device_id_type=MESH
         )
-    for step in distances:
+    for step in reaches:
         ahead, behind = place + step < sp, place >= step
 
         @pl.when(ahead)
@@ -170,10 +169,12 @@
         piece = weight_slice(me, place)
         return to_tp(piece, piece, wy_send.at[o - 1], wy_recv.at[o - 1], far_peer(o))
 
-    def weights_along(o, there, origin):
+    def weights_along(o, origin, up):
         piece = weight_slice(far_owner(o), 2 * origin + side)
+        there = jnp.clip(spot + (1 if up else -1), 0, line - 1)
         return to_sp(
-            piece, piece, wl_send.at[o - 1, there], wl_recv.at[o - 1, origin], 2 * there + side
+            piece, piece, wl_send.at[o - 1, int(up), origin], wl_recv.at[o - 1, origin],
+            2 * there + side,
         )
 
     def weights_pair(o, j, parity):
@@ -186,31 +187,34 @@
         block = wfull.at[:, far_owner(o)]
         return to_tp(block, block, wb_send.at[o - 1], wb_recv.at[o - 1], sibling)
 
-    def both_ways(step, action):
-        for there, valid in ((spot + step, spot + step < line), (spot - step, spot >= step)):
-            @pl.when(valid)
-            def _(there=there):
-                action(jnp.clip(there, 0, line - 1))
+    def pass_on(origin, up, arrived):
+        for o in range(1, chips):
+            if arrived:
+                weights_along(o, origin, up).wait_recv()
+
+            @pl.when(spot + 1 < line if up else spot >= 1)
+            def _(o=o):
+                weights_along(o, origin, up).start()
+
+            if arrived:
+                weights_pair(o, origin, side).start()
 
     def spread_weights():
         for o in range(1, chips):
             weights_across(o).wait_recv()
-        for step in range(1, line):
-            def send(there):
-                for o in range(1, chips):
-                    weights_along(o, there, spot).start()
-
-            both_ways(step, send)
+        pass_on(spot, True, False)
+        pass_on(spot, False, False)
         for o in range(1, chips):
             weights_pair(o, spot, side).start()
 
     def relay_weights(step):
-        def relay(origin):
-            for o in range(1, chips):
-                weights_along(o, origin, origin).wait_recv()
-                weights_pair(o, origin, side).start()
-
-        both_ways(step, relay)
+        @pl.when(spot >= step)
+        def _():
+            pass_on(jnp.maximum(spot - step, 0), True, True)
+
+        @pl.when(spot + step < line)
+        def _():
+            pass_on(jnp.minimum(spot + step, line - 1), False, True)
 
     def collect_weights():
         for o in range(1, chips):
@@ -262,7 +266,7 @@
             for o in range(1, chips):
                 forward(o, first + i).wait_recv()
 
-    def project(first, count):
+    def project_steps(first, count):
         size = count * BLOCK
         here = at(first, count)
         squares = jnp.zeros((size, 1), jnp.float32)
@@ -276,9 +280,11 @@
         gates_s[here, :] = jnp.where(
             lane < heads, jax.nn.sigmoid(raw), -rate_row[...] * softplus
         )
+        yield
         for i in range(PROJECTIONS):
             summed = jnp.dot(full[here, :], w_s[i], preferred_element_type=jnp.float32)
             proj[i, here, :] = (summed * inv_rms).astype(jnp.bfloat16)
+            yield
 
     row_id = lax.broadcasted_iota(jnp.int32, (BLOCK, BLOCK), 0)
     col_id = lax.broadcasted_iota(jnp.int32, (BLOCK, BLOCK), 1)
@@ -319,25 +325,28 @@
             chains.append([h, lower, right, eye - jnp.where(differ == 1, lower, 0.0)])
         return here, c, chains
 
-    def blocks(first, count):
+    def blocks_steps(first, count):
         prepared = [prepare(first + i) for i in range(count)]
+        yield
         size = 2
         while size < BLOCK:
             level = (differ >= size) & (differ < 2 * size)
             parts = [
                 [mm(jnp.where(level, ch[1], 0.0), ch[3]) for ch in item[2]] for item in prepared
             ]
+            yield
             for item, moves in zip(prepared, parts):
                 for ch, moved in zip(item[2], moves):
                     ch[3] = ch[3] - mm(ch[3], moved)
             size *= 2
+            yield
         for here, c, chains in prepared:
             for h, lower, right, inverse in chains:
                 solved = mm(inverse, right)
                 corr_s[h, here, :] = solved[:, :width]
                 lhs_s[h, c, :BLOCK, :] = solved[:, width:].astype(jnp.bfloat16)
 
-    def advance(c):
+    def advance_steps(c):
         here = at(c)
         boths = [mm(lhs_s[h, c], state_ref[h]) for h in range(heads)]
         fresh = []
@@ -348,6 +357,7 @@
                     [-first[:, :width], corr_s[h, here, :] - first[:, width:]], axis=1
                 ).astype(jnp.bfloat16)
             )
+        yield
         for h in range(heads):
             decay = tail_s[h, c][:1, :]
             decay = jnp.concatenate([decay, decay], axis=1)
@@ -356,6 +366,18 @@
             out = boths[h][BLOCK:] + mm(score_s[h, here, :], fresh[h])
             outa_ref[h, here, :] = out[:, :width].astype(jnp.bfloat16)
             outb_ref[h, here, :] = out[:, width:]
+        yield
+
+    def in_turn(*steps):
+        steps = list(steps)
+        while steps:
+            for step in list(steps):
+                if next(step, step) is step:
+                    steps.remove(step)
+
+    def one_by_one(*steps):
+        for step in steps:
+            yield from step
 
     def unit(t):
         value = proj[GLU_VALUE, at(t), :].astype(jnp.float32)
@@ -389,41 +411,40 @@
     for load in w_loads:
         load.wait()
     spread_weights()
-    receive(0, 2)
-    project(0, 2)
-
-    def pair(i, carry):
-        receive(2 * i, 2)
-        relay_weights(i)
-        project(2 * i, 2)
-        blocks(2 * i - 2, 2)
-        for n in range(2):
-            advance(2 * i - 2 + n)
-            unit(2 * i - 2 + n)
-
-        def filter_tile(t, inner):
+
+    def filter_tiles(first, count):
+        for n in range(count):
+            unit(first + n)
+
+        def filter_tile(t, carry):
             @pl.when(t > 0)
             def _():
                 conv(t)
 
-            return inner
-
-        lax.fori_loop(2 * i - 2, 2 * i, filter_tile, 0)
+            return carry
+
+        lax.fori_loop(first, first + count, filter_tile, 0)
+
+    def pair(i, carry):
+        receive(2 * i, 2)
+        in_turn(project_steps(2 * i, 2))
+        relay_weights(i + 1)
+        in_turn(blocks_steps(2 * i, 2))
+        in_turn(one_by_one(advance_steps(2 * i), advance_steps(2 * i + 1)))
+        filter_tiles(2 * i, 2)
         return carry
 
-    paired = tiles // 2 - 1
-    lax.fori_loop(1, paired, pair, 0)
-    for step in range(paired, line):
+    tail = tiles - 4
+    lax.fori_loop(0, tail // 2, pair, 0)
+    receive(tail, 2)
+    in_turn(project_steps(tail, 2))
+    filter_tiles(tail, 2)
+    for step in range(tail // 2 + 1, line):
         relay_weights(step)
-    tail = 2 * paired
-    receive(tail, 1)
-    project(tail, 1)
-    blocks(tail - 2, 2)
+    receive(tail + 2, 2)
+    in_turn(blocks_steps(tail, 2), project_steps(tail + 2, 2))
     for n in range(2):
-        advance(tail - 2 + n)
-    receive(tail + 1, 1)
-    project(tail + 1, 1)
-    units = unit(tail + 1)
+        units = unit(tail + 2 + n)
     halo_out[...] = units[BLOCK - halo :, :]
     halo_copy = to_sp(
         halo_out, halo_in, halo_send.at[0], halo_recv.at[0], jnp.minimum(place + 1, sp - 1)
@@ -433,9 +454,10 @@
     def _():
         halo_copy.start()
 
-    blocks(tail, 2)
-    for n in range(2):
-        advance(tail + n)
+    in_turn(
+        blocks_steps(tail + 2, 2), one_by_one(advance_steps(tail), advance_steps(tail + 1))
+    )
+    in_turn(one_by_one(advance_steps(tail + 2), advance_steps(tail + 3)))
     final_ref[...] = state_ref[...].astype(jnp.bfloat16)
 
     def carry_copy(i, h):
@@ -481,9 +503,7 @@
     for h in range(heads):
         send_carry(0, h)
 
-    for n in range(3):
-        unit(tail - 2 + n)
-    lax.fori_loop(tail - 2, tail + 2, conv, 0)
+    lax.fori_loop(tail + 2, tail + 4, conv, 0)
 
     @pl.when(place >= 1)
     def _():
@@ -565,12 +585,6 @@
 
     cuts = out_ref.shape[1] // OUT_CUT
     sources = [sibling] + far_targets
-    for source in sources:
-        mixed_wait(1, source)
-    weights_beside().wait_recv()
-    for o in range(1, chips):
-        weights_forward(o).wait_recv()
-
     def conv_part(n, carry):
         total = jnp.dot(
             mixed_out[1, me], wfull[1, me, :, out_columns(n)], preferred_element_type=jnp.float32
@@ -583,7 +597,6 @@
         acc_s[:, out_columns(n)] = total
         return carry
 
-    lax.fori_loop(0, cuts, conv_part, 0)
 
     carried = []
     for h in range(heads):
@@ -616,6 +629,12 @@
         attend(target)
         mixed_copy(0, target).start()
     attend(me)
+    for source in sources:
+        mixed_wait(1, source)
+    weights_beside().wait_recv()
+    for o in range(1, chips):
+        weights_forward(o).wait_recv()
+    lax.fori_loop(0, cuts, conv_part, 0)
     mixed_wait(0, sibling)
 
     def near_part(n, carry):
@@ -657,12 +676,13 @@
         weights_forward(o).wait_send()
         for j in range(line):
             weights_pair(o, j, side).wait_send()
-    for step in range(1, line):
-        def sent(there):
-            for o in range(1, chips):
-                weights_along(o, there, spot).wait_send()
-
-        both_ways(step, sent)
+    for origin in range(line):
+        for up in (True, False):
+            @pl.when((origin <= spot) & (spot + 1 < line) if up else (origin >= spot) & (spot >= 1))
+            def _(origin=origin, up=up):
+                for o in range(1, chips):
+                    weights_along(o, origin, up).wait_send()
+
     for i in range(last + 1):
         @pl.when(place + reaches[i] < sp)
         def _(i=i):
@@ -706,7 +726,7 @@
     return pl.pallas_call(
         functools.partial(layer_kernel, heads, width),
         out_shape=jax.ShapeDtypeStruct((slot, columns), bf16),
-        in_specs=[pl.BlockSpec(memory_space=pl.ANY)] * 17,
+        in_specs=[pl.BlockSpec(memory_space=pltpu.HBM)] * 17,
         out_specs=pl.BlockSpec(memory_space=pltpu.VMEM),
         scratch_shapes=[
             vmem((rows, features), bf16),
@@ -759,7 +779,7 @@
             dma((1,)),
             dma((others,)),
             dma((others,)),
-            dma((others, line)),
+            dma((others, 2, line)),
             dma((others, line)),
             dma((others, line)),
             dma((others, line)),
@@ -775,15 +795,20 @@
             dma((2, tp)),
         ],
         compiler_params=pltpu.CompilerParams(
-            collective_id=0, has_side_effects=True, vmem_limit_bytes=60 * 1024 * 1024
+            collective_id=0, has_side_effects=True, vmem_limit_bytes=46 * 1024 * 1024
         ),
         cost_estimate=pl.CostEstimate(
             flops=20_000_000_000, bytes_accessed=20_000_000, transcendentals=0
         ),
         name="layer",
     )(
-        tokens, *weights, w_beta, w_decay, decay_log, gain, taps, ln_gain, ln_shift,
-        out_delta, out_conv,
+        *(
+            pltpu.with_memory_space_constraint(x, pltpu.HBM)
+            for x in (
+                tokens, *weights, w_beta, w_decay, decay_log, gain, taps, ln_gain, ln_shift,
+                out_delta, out_conv,
+            )
+        )
     )
 
 

time: 85.8 us -> 69.5 us (0.81)
  Pallas kernels: 82.8 us -> 67.5 us
  local copies, waits for them, and re-layouts: 2.3 us -> 0.97 us
    pallas_call x1, Pallas kernels: 82.8 us -> 67.5 us  [layer(): pl.pallas_call(functools.partial(layer_kernel, heads, width), out_shape=j...]
    unnamed x1, local copies, waits for them, and re-layouts: 2.3 us -> 0.97 us
where the time goes in v3:
time: 69.5 us; the launch traced here: 68.4 us
  Pallas kernels  67.5 us (97%)
  local copies, waits for them, and re-layouts  0.97 us (1%)
    pallas_call x1, Pallas kernels, layer(): pl.pallas_call(functools.partial(layer_kernel, heads, width), out_shape=j...  67.5 us

profile of v3, /device:TPU:9, one launch (start us, length us, event | category | flops | bytes accessed | tf_op | source)
XLA Modules:
  0.0 68.4 jit_solution(13434269838244337209)
XLA Ops:
  0.0 67.5 %layer.1 = bf16[256,2048]{1,0:T(8,128)(2,1)S(1)} custom-call(bf16[1024,512]{1,0:T(8,128)(2,1)} %tok_hbm.1, bf16[2048,256]{1,0:T(8,128)(2,1)} %wq_hbm.1, bf16[2048,256]{1,0:T(8,128)(2,1)} %wk_hbm.1, bf16[2048,256]{1,0:T(8,128)(2,1)} %wv_hbm.1, bf16[2048,256]{1,0:T(8,128)(2,1)} %wdg_hbm.1, bf16[2048,256]{1,0:T(8,128)(2,1)} %wgv_hbm.1, ...), custom_call_target="tpu_custom_call" | custom-call | flops 20000000000 | bytes 20000000 | tf_op jit(solution)/shard_map/layer/pallas_call | solution.py:726
  67.5 1.0 %copy.19 = bf16[256,2048]{1,0:T(8,128)(2,1)} copy(bf16[256,2048]{1,0:T(8,128)(2,1)S(1)} %layer.1) | data formatting | bytes 2097152

commit v4 on v3

--- a/solution.py
+++ b/solution.py
@@ -93,8 +93,7 @@
             (taps_hbm, taps_s), (ln_gain_hbm, ln_gain_ref), (ln_shift_hbm, ln_shift_ref),
         ))
     ]
-    token_loads[0].start()
-    for load in out_loads + token_loads[1:] + small_loads + w_loads:
+    for load in out_loads + token_loads + small_loads:
         load.start()
 
     reaches = [1]
@@ -231,7 +230,8 @@
         for o in range(1, chips):
             across(o, r).start()
         beside(r).start()
-    weights_beside().start()
+    for load in w_loads:
+        load.start()
     for load in small_loads:
         load.wait()
 
@@ -256,11 +256,13 @@
     ).astype(jnp.bfloat16)
     taps_ref[...] = taps_s[...].astype(jnp.float32)
 
-    def receive(first, count):
+    def pass_tokens(first, count):
         for i in range(count):
             for o in range(1, chips):
                 across(o, first + i).wait_recv()
                 forward(o, first + i).start()
+
+    def take_tokens(first, count):
         for i in range(count):
             beside(first + i).wait_recv()
             for o in range(1, chips):
@@ -390,7 +392,7 @@
             ]
         return units
 
-    def conv(t, carry=0):
+    def conv_steps(t):
         first = jnp.zeros((BLOCK, 1), jnp.float32)
         second = jnp.zeros((BLOCK, 1), jnp.float32)
         for g in range(groups):
@@ -402,16 +404,19 @@
             filtered[g, at(t), :] = total
             first = first + jnp.sum(total, axis=1, keepdims=True)
             second = second + jnp.sum(total * total, axis=1, keepdims=True)
+            yield
         lane = lax.broadcasted_iota(jnp.int32, (BLOCK, BLOCK), 1)
         sums_out[t] = jnp.where(lane == 0, first, jnp.where(lane == 1, second, 0.0)).T[:8, :]
-        return carry
+        yield
+
+    def conv(t):
+        for step in conv_steps(t):
+            pass
 
     for h in range(heads):
         state_ref[h] = jnp.concatenate([eye, jnp.zeros((width, width), jnp.float32)], axis=1)
     for load in w_loads:
         load.wait()
-    spread_weights()
-
     def filter_tiles(first, count):
         for n in range(count):
             unit(first + n)
@@ -425,24 +430,51 @@
 
         lax.fori_loop(first, first + count, filter_tile, 0)
 
+    tail = tiles - 4
+    ln_parts = (pl.ds(2, tail), pl.ds(0, 2), pl.ds(tail + 2, 2))
+
+    def ln_copy(step, which):
+        cut = ln_parts[which]
+        return to_tp(
+            sums_out.at[cut], sums_in.at[step - 1, cut],
+            ln_send.at[step - 1, which], ln_recv.at[step - 1, which], lax.rem(me + step, tp),
+        )
+
+    spread_weights()
+    pass_tokens(0, 2)
+    take_tokens(0, 2)
+    in_turn(project_steps(0, 2))
+    relay_weights(1)
+    filter_tiles(0, 2)
+    in_turn(blocks_steps(0, 2))
+    in_turn(one_by_one(advance_steps(0), advance_steps(1)))
+    pass_tokens(2, 2)
+
     def pair(i, carry):
-        receive(2 * i, 2)
+        take_tokens(2 * i, 2)
         in_turn(project_steps(2 * i, 2))
+        filter_tiles(2 * i, 2)
+        pass_tokens(2 * i + 2, 2)
         relay_weights(i + 1)
-        in_turn(blocks_steps(2 * i, 2))
-        in_turn(one_by_one(advance_steps(2 * i), advance_steps(2 * i + 1)))
-        filter_tiles(2 * i, 2)
         return carry
 
-    tail = tiles - 4
-    lax.fori_loop(0, tail // 2, pair, 0)
-    receive(tail, 2)
+    lax.fori_loop(1, tail // 2, pair, 0)
+    take_tokens(tail, 2)
     in_turn(project_steps(tail, 2))
     filter_tiles(tail, 2)
-    for step in range(tail // 2 + 1, line):
-        relay_weights(step)
-    receive(tail + 2, 2)
-    in_turn(blocks_steps(tail, 2), project_steps(tail + 2, 2))
+    for step in range(1, tp):
+        ln_copy(step, 0).start()
+    in_turn(blocks_steps(2, tail))
+    pass_tokens(tail + 2, 2)
+    relay_weights(tail // 2 + 1)
+    take_tokens(tail + 2, 1)
+    in_turn(
+        project_steps(tail + 2, 1),
+        one_by_one(*(advance_steps(c) for c in range(2, tail + 2))),
+    )
+    take_tokens(tail + 3, 1)
+    weights_beside().start()
+    in_turn(project_steps(tail + 3, 1))
     for n in range(2):
         units = unit(tail + 2 + n)
     halo_out[...] = units[BLOCK - halo :, :]
@@ -454,105 +486,118 @@
     def _():
         halo_copy.start()
 
-    in_turn(
-        blocks_steps(tail + 2, 2), one_by_one(advance_steps(tail), advance_steps(tail + 1))
-    )
+    in_turn(blocks_steps(tail + 2, 2), one_by_one(conv_steps(tail + 2), conv_steps(tail + 3)))
+    for step in range(tail // 2 + 2, line):
+        relay_weights(step)
+
+    @pl.when(place >= 1)
+    def _():
+        halo_copy.wait_recv()
+
+    @pl.when(place < 1)
+    def _():
+        halo_in[...] = jnp.zeros(halo_in.shape, jnp.bfloat16)
+
+    before = halo_in[...].astype(jnp.float32)
+    for g in range(groups):
+        padded[g, :halo, :] = before[:, g * lanes : (g + 1) * lanes]
+    conv(0)
+
+    for step in range(1, tp):
+        ln_copy(step, 1).start()
+        ln_copy(step, 2).start()
     in_turn(one_by_one(advance_steps(tail + 2), advance_steps(tail + 3)))
     final_ref[...] = state_ref[...].astype(jnp.bfloat16)
 
-    def carry_copy(i, h):
-        cut = slice(width, 2 * width) if i == last else slice(0, 2 * width)
+    shift, offset = slice(0, width), slice(width, 2 * width)
+
+    def carry_copy(i, h, cut):
         source = final_ref if i == 0 else sent_s.at[i - 1]
+        which = 0 if cut is shift else 1
         return to_sp(
-            source.at[h, :, cut], far_s.at[i, h, :, cut], far_send.at[i, h], far_recv.at[i, h],
+            source.at[h, :, cut], far_s.at[i, h, :, cut],
+            far_send.at[i, h, which], far_recv.at[i, h, which],
             jnp.minimum(place + reaches[i], sp - 1),
         )
 
-    def send_carry(i, h):
+    def send_carry(i, h, cut):
+        if i == last and cut is shift:
+            return
+
         @pl.when(place + reaches[i] < sp)
         def _():
-            carry_copy(i, h).start()
-
-    def take_carry(i, h):
+            carry_copy(i, h, cut).start()
+
+    def take_carry(i, h, cut):
         @pl.when(place >= reaches[i])
         def _():
-            carry_copy(i, h).wait_recv()
+            carry_copy(i, h, cut).wait_recv()
 
         @pl.when(place < reaches[i])
         def _():
-            far_s[i, h] = jnp.zeros((width, 2 * width), jnp.bfloat16)
-
-    def combine(later, earlier):
-        moved = mm(later[:, :width], earlier)
-        return jnp.concatenate(
-            [moved[:, :width], moved[:, width:] + later[:, width:].astype(jnp.float32)], axis=1
-        )
+            far_s[i, h, :, cut] = jnp.zeros((width, width), jnp.bfloat16)
 
     def exchange(i):
+        own = final_ref if i == 0 else sent_s.at[i - 1]
         for h in range(heads):
-            take_carry(i, h)
-            own = final_ref[h] if i == 0 else sent_s[i - 1, h]
-            sent_s[i, h] = combine(own, far_s[i, h]).astype(jnp.bfloat16)
-            send_carry(i + 1, h)
+            take_carry(i, h, offset)
+            later = mm(own[h, :, shift], far_s[i, h, :, offset])
+            later = later + own[h, :, offset].astype(jnp.float32)
+            sent_s[i, h, :, offset] = later.astype(jnp.bfloat16)
+            send_carry(i + 1, h, offset)
+        for h in range(heads):
+            take_carry(i, h, shift)
+            sent_s[i, h, :, shift] = mm(own[h, :, shift], far_s[i, h, :, shift]).astype(
+                jnp.bfloat16
+            )
+            send_carry(i + 1, h, shift)
         for h in range(heads):
             if i == 0:
                 window_s[h] = far_s[i, h].astype(jnp.float32)
             else:
-                window_s[h] = combine(window_s[h], far_s[i, h])
+                window = window_s[h]
+                moved = mm(window[:, shift], far_s[i, h])
+                window_s[h] = jnp.concatenate(
+                    [moved[:, shift], moved[:, offset] + window[:, offset]], axis=1
+                )
 
     for h in range(heads):
-        send_carry(0, h)
-
-    lax.fori_loop(tail + 2, tail + 4, conv, 0)
-
-    @pl.when(place >= 1)
-    def _():
-        halo_copy.wait_recv()
-
-    @pl.when(place < 1)
-    def _():
-        halo_in[...] = jnp.zeros(halo_in.shape, jnp.bfloat16)
-
-    before = halo_in[...].astype(jnp.float32)
-    for g in range(groups):
-        padded[g, :halo, :] = before[:, g * lanes : (g + 1) * lanes]
-    conv(0)
-
-    def ln_copy(step):
-        return to_tp(
-            sums_out, sums_in.at[step - 1], ln_send.at[step - 1], ln_recv.at[step - 1],
-            lax.rem(me + step, tp),
-        )
+        send_carry(0, h, offset)
+    for h in range(heads):
+        send_carry(0, h, shift)
+    collect_weights()
+
 
     for step in range(1, tp):
-        ln_copy(step).start()
-    if last > 0:
-        exchange(0)
-    for step in range(1, tp):
-        ln_copy(step).wait_recv()
+        ln_copy(step, 0).wait_recv()
     channels = groups * lanes * tp
     per = tiles // tp
 
+    def mixed_part(buffer, owner, kind):
+        if kind == heads:
+            return buffer.at[1, owner]
+        return buffer.at[0, owner, :, kind * width : (kind + 1) * width]
+
     def mixed_copy(kind, there):
         return to_tp(
-            mixed_out.at[kind, there], mixed_in.at[kind, me],
+            mixed_part(mixed_out, there, kind), mixed_part(mixed_in, me, kind),
             mix_send.at[kind, there], mix_recv.at[kind, me], there,
         )
 
     def mixed_wait(kind, source):
+        part_in = mixed_part(mixed_in, source, kind)
         to_tp(
-            mixed_out.at[kind, source], mixed_in.at[kind, source],
-            mix_send.at[kind, source], mix_recv.at[kind, source], source,
+            part_in, part_in, mix_send.at[kind, source], mix_recv.at[kind, source], source
         ).wait_recv()
 
     far_targets = [
         lax.rem(chip + o, chips) * 2 + lax.rem(core + c, 2) for o in range(1, chips) for c in (0, 1)
     ]
 
-    def norm(target):
-        def tile(i, carry):
+    def norm(targets):
+        for target, i in [(target, i) for target in targets for i in range(per)]:
             t = target * per + i
-            here = pl.ds(pl.multiple_of(i * BLOCK, BLOCK), BLOCK)
+            here = pl.ds(i * BLOCK, BLOCK)
             sums = sums_out[t]
             for step in range(1, tp):
                 sums = sums + sums_in[step - 1, t]
@@ -568,102 +613,111 @@
                 mixed_out[1, target, here, cut] = (
                     jax.nn.silu(normed) * jax.nn.silu(gate)
                 ).astype(jnp.bfloat16)
-            return carry
-
-        lax.fori_loop(0, per, tile, 0)
-
-    for target in far_targets + [sibling]:
-        norm(target)
-        mixed_copy(1, target).start()
-    norm(me)
+
+    early = [t for t in range(tp) if t * per >= 2 and (t + 1) * per <= tail + 2]
+
+    def norm_far(target):
+        @pl.when(target // 2 != chip)
+        def _():
+            norm([target])
+            mixed_copy(heads, target).start()
+
+    for target in early:
+        norm_far(target)
+    if last > 0:
+        exchange(0)
+    for step in range(1, tp):
+        ln_copy(step, 1).wait_recv()
+        ln_copy(step, 2).wait_recv()
+    for target in range(tp):
+        if target not in early:
+            norm_far(target)
+    norm([sibling])
+    mixed_copy(heads, sibling).start()
+    norm([me])
     for i in range(1, last):
         exchange(i)
-    collect_weights()
 
     def out_columns(n):
         return pl.ds(pl.multiple_of(n * OUT_CUT, OUT_CUT), OUT_CUT)
 
     cuts = out_ref.shape[1] // OUT_CUT
     sources = [sibling] + far_targets
-    def conv_part(n, carry):
-        total = jnp.dot(
-            mixed_out[1, me], wfull[1, me, :, out_columns(n)], preferred_element_type=jnp.float32
-        )
-        for source in sources:
-            total = total + jnp.dot(
-                mixed_in[1, source], wfull[1, source, :, out_columns(n)],
-                preferred_element_type=jnp.float32,
-            )
-        acc_s[:, out_columns(n)] = total
-        return carry
-
-
-    carried = []
-    for h in range(heads):
-        take_carry(last, h)
-        earlier = far_s[last, h, :, width:]
-        if last > 0:
-            window = window_s[h]
-            earlier = mm(window[:, :width], earlier) + window[:, width:]
-        carried.append(earlier.astype(jnp.bfloat16))
-
-    def attend(target):
-        def tile(i, carry):
-            t = target * per + i
-            here = pl.ds(pl.multiple_of(i * BLOCK, BLOCK), BLOCK)
-            for h in range(heads):
-                cut = slice(h * width, (h + 1) * width)
-                result = outb_ref[h, at(t), :] + mm(outa_ref[h, at(t), :], carried[h])
-                result = result * lax.rsqrt(
-                    jnp.mean(result * result, axis=-1, keepdims=True) + TINY_NORM
+
+    def product(terms, head=None, start=False, close=False):
+        def part(n, carry):
+            total = jnp.zeros((out_ref.shape[0], OUT_CUT), jnp.float32)
+            for kind, source, rows_ref in terms:
+                total = total + jnp.dot(
+                    rows_ref[kind, source], wfull[kind, source, :, out_columns(n)],
+                    preferred_element_type=jnp.float32,
                 )
-                gate = proj[DELTA_GATE, at(t), cut].astype(jnp.float32)
-                mixed_out[0, target, here, cut] = (
-                    result * gain_ref[...] * jax.nn.silu(gate)
-                ).astype(jnp.bfloat16)
-            return carry
-
-        lax.fori_loop(0, per, tile, 0)
-
-    for target in far_targets + [sibling]:
-        attend(target)
-        mixed_copy(0, target).start()
-    attend(me)
-    for source in sources:
-        mixed_wait(1, source)
-    weights_beside().wait_recv()
-    for o in range(1, chips):
-        weights_forward(o).wait_recv()
-    lax.fori_loop(0, cuts, conv_part, 0)
-    mixed_wait(0, sibling)
-
-    def near_part(n, carry):
-        total = jnp.dot(
-            mixed_out[0, me], wfull[0, me, :, out_columns(n)], preferred_element_type=jnp.float32
-        )
-        total = total + jnp.dot(
-            mixed_in[0, sibling], wfull[0, sibling, :, out_columns(n)],
-            preferred_element_type=jnp.float32,
-        )
-        acc_s[:, out_columns(n)] = acc_s[:, out_columns(n)] + total
-        return carry
-
-    lax.fori_loop(0, cuts, near_part, 0)
-    for index, source in enumerate(far_targets):
-        mixed_wait(0, source)
-
-        def far_part(n, carry, source=source, closing=index + 1 == len(far_targets)):
-            total = acc_s[:, out_columns(n)] + jnp.dot(
-                mixed_in[0, source], wfull[0, source, :, out_columns(n)],
-                preferred_element_type=jnp.float32,
-            )
-            if closing:
+            if head is not None:
+                cut = slice(head * width, (head + 1) * width)
+                total = total + jnp.dot(
+                    jnp.concatenate([mixed_in[0, t, :, cut] for t in far_targets], axis=1),
+                    jnp.concatenate(
+                        [wfull[0, t, cut, out_columns(n)] for t in far_targets], axis=0
+                    ),
+                    preferred_element_type=jnp.float32,
+                )
+            if not start:
+                total = total + acc_s[:, out_columns(n)]
+            if close:
                 out_ref[:, out_columns(n)] = total.astype(jnp.bfloat16)
             else:
                 acc_s[:, out_columns(n)] = total
             return carry
 
-        lax.fori_loop(0, cuts, far_part, 0)
+        lax.fori_loop(0, cuts, part, 0)
+
+    def state_before(h):
+        take_carry(last, h, offset)
+        earlier = far_s[last, h, :, offset]
+        if last > 0:
+            window = window_s[h]
+            earlier = mm(window[:, shift], earlier) + window[:, offset]
+        return earlier.astype(jnp.bfloat16)
+
+    def attend(targets, h, carried):
+        cut = slice(h * width, (h + 1) * width)
+        for target, i in [(target, i) for target in targets for i in range(per)]:
+            t = target * per + i
+            here = pl.ds(i * BLOCK, BLOCK)
+            result = outb_ref[h, at(t), :] + mm(outa_ref[h, at(t), :], carried)
+            result = result * lax.rsqrt(
+                jnp.mean(result * result, axis=-1, keepdims=True) + TINY_NORM
+            )
+            gate = proj[DELTA_GATE, at(t), cut].astype(jnp.float32)
+            mixed_out[0, target, here, cut] = (
+                result * gain_ref[...] * jax.nn.silu(gate)
+            ).astype(jnp.bfloat16)
+
+    weights_beside().wait_recv()
+    mixed_wait(heads, sibling)
+    product([(1, me, mixed_out), (1, sibling, mixed_in)], start=True)
+    carried = []
+    for h in range(heads):
+        carried.append(state_before(h))
+        attend(far_targets, h, carried[h])
+        for target in far_targets:
+            mixed_copy(h, target).start()
+    for h in range(heads):
+        attend([sibling, me], h, carried[h])
+    for h in range(heads):
+        mixed_copy(h, sibling).start()
+    for source in far_targets:
+        mixed_wait(heads, source)
+    for o in range(1, chips):
+        weights_forward(o).wait_recv()
+    product([(1, source, mixed_in) for source in far_targets])
+    for h in range(heads):
+        mixed_wait(h, sibling)
+    product([(0, me, mixed_out), (0, sibling, mixed_in)])
+    for h in range(heads):
+        for source in far_targets:
+            mixed_wait(h, source)
+        product([], head=h, close=h + 1 == heads)
 
     for r in range(tiles):
         for o in range(1, chips):
@@ -687,15 +741,18 @@
         @pl.when(place + reaches[i] < sp)
         def _(i=i):
             for h in range(heads):
-                carry_copy(i, h).wait_send()
+                carry_copy(i, h, offset).wait_send()
+                if i < last:
+                    carry_copy(i, h, shift).wait_send()
 
     @pl.when(place + 1 < sp)
     def _():
         halo_copy.wait_send()
 
     for step in range(1, tp):
-        ln_copy(step).wait_send()
-    for kind in range(2):
+        for which in range(3):
+            ln_copy(step, which).wait_send()
+    for kind in range(heads + 1):
         for target in sources:
             mixed_copy(kind, target).wait_send()
 
@@ -785,14 +842,14 @@
             dma((others, line)),
             dma((others,)),
             dma((others,)),
-            dma((steps, heads)),
-            dma((steps, heads)),
+            dma((steps, heads, 2)),
+            dma((steps, heads, 2)),
             dma((1,)),
             dma((1,)),
-            dma((tp - 1,)),
-            dma((tp - 1,)),
-            dma((2, tp)),
-            dma((2, tp)),
+            dma((tp - 1, 3)),
+            dma((tp - 1, 3)),
+            dma((heads + 1, tp)),
+            dma((heads + 1, tp)),
         ],
         compiler_params=pltpu.CompilerParams(
             collective_id=0, has_side_effects=True, vmem_limit_bytes=46 * 1024 * 1024

time: 69.5 us -> 65.6 us (0.944); the launches traced: 68.4 us -> 65.5 us
  Pallas kernels: 67.5 us -> 64.5 us
    pallas_call x1, Pallas kernels: 67.5 us -> 64.5 us  [layer(): pl.pallas_call(functools.partial(layer_kernel, heads, width), out_shape=j...]
where the time goes in v4:
time: 65.6 us; the launch traced here: 65.5 us
  Pallas kernels  64.5 us (98%)
  local copies, waits for them, and re-layouts  0.97 us (1%)
    pallas_call x1, Pallas kernels, layer(): pl.pallas_call(functools.partial(layer_kernel, heads, width), out_shape=j...  64.5 us

profile of v4, /device:TPU:9, one launch (start us, length us, event | category | flops | bytes accessed | tf_op | source)
XLA Modules:
  0.0 65.5 jit_solution(17012383083320589516)
XLA Ops:
  0.0 64.5 %layer.1 = bf16[256,2048]{1,0:T(8,128)(2,1)S(1)} custom-call(bf16[1024,512]{1,0:T(8,128)(2,1)} %tok_hbm.1, bf16[2048,256]{1,0:T(8,128)(2,1)} %wq_hbm.1, bf16[2048,256]{1,0:T(8,128)(2,1)} %wk_hbm.1, bf16[2048,256]{1,0:T(8,128)(2,1)} %wv_hbm.1, bf16[2048,256]{1,0:T(8,128)(2,1)} %wdg_hbm.1, bf16[2048,256]{1,0:T(8,128)(2,1)} %wgv_hbm.1, ...), custom_call_target="tpu_custom_call" | custom-call | flops 20000000000 | bytes 20000000 | tf_op jit(solution)/shard_map/layer/pallas_call | solution.py:783
  64.5 1.0 %copy.19 = bf16[256,2048]{1,0:T(8,128)(2,1)} copy(bf16[256,2048]{1,0:T(8,128)(2,1)S(1)} %layer.1) | data formatting | bytes 2097152

commit v5 on v4

--- a/solution.py
+++ b/solution.py
@@ -467,14 +467,9 @@
     in_turn(blocks_steps(2, tail))
     pass_tokens(tail + 2, 2)
     relay_weights(tail // 2 + 1)
-    take_tokens(tail + 2, 1)
-    in_turn(
-        project_steps(tail + 2, 1),
-        one_by_one(*(advance_steps(c) for c in range(2, tail + 2))),
-    )
-    take_tokens(tail + 3, 1)
+    take_tokens(tail + 2, 2)
     weights_beside().start()
-    in_turn(project_steps(tail + 3, 1))
+    in_turn(project_steps(tail + 2, 2))
     for n in range(2):
         units = unit(tail + 2 + n)
     halo_out[...] = units[BLOCK - halo :, :]
@@ -486,26 +481,11 @@
     def _():
         halo_copy.start()
 
-    in_turn(blocks_steps(tail + 2, 2), one_by_one(conv_steps(tail + 2), conv_steps(tail + 3)))
+    in_turn(
+        blocks_steps(tail + 2, 2), one_by_one(*(advance_steps(c) for c in range(2, tail + 2)))
+    )
     for step in range(tail // 2 + 2, line):
         relay_weights(step)
-
-    @pl.when(place >= 1)
-    def _():
-        halo_copy.wait_recv()
-
-    @pl.when(place < 1)
-    def _():
-        halo_in[...] = jnp.zeros(halo_in.shape, jnp.bfloat16)
-
-    before = halo_in[...].astype(jnp.float32)
-    for g in range(groups):
-        padded[g, :halo, :] = before[:, g * lanes : (g + 1) * lanes]
-    conv(0)
-
-    for step in range(1, tp):
-        ln_copy(step, 1).start()
-        ln_copy(step, 2).start()
     in_turn(one_by_one(advance_steps(tail + 2), advance_steps(tail + 3)))
     final_ref[...] = state_ref[...].astype(jnp.bfloat16)
 
@@ -566,8 +546,25 @@
     for h in range(heads):
         send_carry(0, h, shift)
     collect_weights()
-
-
+    conv(tail + 2)
+    conv(tail + 3)
+
+    @pl.when(place >= 1)
+    def _():
+        halo_copy.wait_recv()
+
+    @pl.when(place < 1)
+    def _():
+        halo_in[...] = jnp.zeros(halo_in.shape, jnp.bfloat16)
+
+    before = halo_in[...].astype(jnp.float32)
+    for g in range(groups):
+        padded[g, :halo, :] = before[:, g * lanes : (g + 1) * lanes]
+    conv(0)
+
+    for step in range(1, tp):
+        ln_copy(step, 1).start()
+        ln_copy(step, 2).start()
     for step in range(1, tp):
         ln_copy(step, 0).wait_recv()
     channels = groups * lanes * tp
@@ -669,7 +666,7 @@
                 acc_s[:, out_columns(n)] = total
             return carry
 
-        lax.fori_loop(0, cuts, part, 0)
+        lax.fori_loop(0, cuts, part, 0, unroll=close)
 
     def state_before(h):
         take_carry(last, h, offset)
@@ -693,9 +690,6 @@
                 result * gain_ref[...] * jax.nn.silu(gate)
             ).astype(jnp.bfloat16)
 
-    weights_beside().wait_recv()
-    mixed_wait(heads, sibling)
-    product([(1, me, mixed_out), (1, sibling, mixed_in)], start=True)
     carried = []
     for h in range(heads):
         carried.append(state_before(h))
@@ -706,6 +700,9 @@
         attend([sibling, me], h, carried[h])
     for h in range(heads):
         mixed_copy(h, sibling).start()
+    weights_beside().wait_recv()
+    mixed_wait(heads, sibling)
+    product([(1, me, mixed_out), (1, sibling, mixed_in)], start=True)
     for source in far_targets:
         mixed_wait(heads, source)
     for o in range(1, chips):
@@ -714,11 +711,6 @@
     for h in range(heads):
         mixed_wait(h, sibling)
     product([(0, me, mixed_out), (0, sibling, mixed_in)])
-    for h in range(heads):
-        for source in far_targets:
-            mixed_wait(h, source)
-        product([], head=h, close=h + 1 == heads)
-
     for r in range(tiles):
         for o in range(1, chips):
             across(o, r).wait_send()
@@ -752,6 +744,11 @@
     for step in range(1, tp):
         for which in range(3):
             ln_copy(step, which).wait_send()
+    for h in range(heads):
+        for source in far_targets:
+            mixed_wait(h, source)
+        product([], head=h, close=h + 1 == heads)
+
     for kind in range(heads + 1):
         for target in sources:
             mixed_copy(kind, target).wait_send()

time: 65.6 us -> 64.1 us (0.977)
  the two profiles are of different devices: /device:TPU:9 before, /device:TPU:27 now
where the time goes in v5:
time: 64.1 us; the launch traced here: 64 us
  Pallas kernels  63 us (98%)
  local copies, waits for them, and re-layouts  0.97 us (2%)
    pallas_call x1, Pallas kernels, layer(): pl.pallas_call(functools.partial(layer_kernel, heads, width), out_shape=j...  63 us

profile of v5, /device:TPU:27, one launch (start us, length us, event | category | flops | bytes accessed | tf_op | source)
XLA Modules:
  0.0 64.0 jit_solution(9527279798867520326)
XLA Ops:
  0.0 63.0 %layer.1 = bf16[256,2048]{1,0:T(8,128)(2,1)S(1)} custom-call(bf16[1024,512]{1,0:T(8,128)(2,1)} %tok_hbm.1, bf16[2048,256]{1,0:T(8,128)(2,1)} %wq_hbm.1, bf16[2048,256]{1,0:T(8,128)(2,1)} %wk_hbm.1, bf16[2048,256]{1,0:T(8,128)(2,1)} %wv_hbm.1, bf16[2048,256]{1,0:T(8,128)(2,1)} %wdg_hbm.1, bf16[2048,256]{1,0:T(8,128)(2,1)} %wgv_hbm.1, ...), custom_call_target="tpu_custom_call" | custom-call | flops 20000000000 | bytes 20000000 | tf_op jit(solution)/shard_map/layer/pallas_call | solution.py:780
  63.0 1.0 %copy.19 = bf16[256,2048]{1,0:T(8,128)(2,1)} copy(bf16[256,2048]{1,0:T(8,128)(2,1)S(1)} %layer.1) | data formatting | bytes 2097152

commit v6 on v5

--- a/solution.py
+++ b/solution.py
@@ -629,11 +629,11 @@
     for target in range(tp):
         if target not in early:
             norm_far(target)
+    for i in range(1, last):
+        exchange(i)
     norm([sibling])
     mixed_copy(heads, sibling).start()
     norm([me])
-    for i in range(1, last):
-        exchange(i)
 
     def out_columns(n):
         return pl.ds(pl.multiple_of(n * OUT_CUT, OUT_CUT), OUT_CUT)
@@ -666,7 +666,7 @@
                 acc_s[:, out_columns(n)] = total
             return carry
 
-        lax.fori_loop(0, cuts, part, 0, unroll=close)
+        lax.fori_loop(0, cuts, part, 0, unroll=True)
 
     def state_before(h):
         take_carry(last, h, offset)
@@ -700,14 +700,14 @@
         attend([sibling, me], h, carried[h])
     for h in range(heads):
         mixed_copy(h, sibling).start()
-    weights_beside().wait_recv()
-    mixed_wait(heads, sibling)
-    product([(1, me, mixed_out), (1, sibling, mixed_in)], start=True)
     for source in far_targets:
         mixed_wait(heads, source)
     for o in range(1, chips):
         weights_forward(o).wait_recv()
-    product([(1, source, mixed_in) for source in far_targets])
+    product([(1, source, mixed_in) for source in far_targets], start=True)
+    weights_beside().wait_recv()
+    mixed_wait(heads, sibling)
+    product([(1, me, mixed_out), (1, sibling, mixed_in)])
     for h in range(heads):
         mixed_wait(h, sibling)
     product([(0, me, mixed_out), (0, sibling, mixed_in)])

time: 64.1 us -> 63.7 us (level)
  the two profiles are of different devices: /device:TPU:27 before, /device:TPU:0 now
where the time goes in v6:
time: 63.7 us; the launch traced here: 63.6 us
  Pallas kernels  62.6 us (98%)
  local copies, waits for them, and re-layouts  0.97 us (2%)
    pallas_call x1, Pallas kernels, layer(): pl.pallas_call(functools.partial(layer_kernel, heads, width), out_shape=j...  62.6 us

profile of v6, /device:TPU:0, one launch (start us, length us, event | category | flops | bytes accessed | tf_op | source)
XLA Modules:
  0.0 63.6 jit_solution(16832638318667893853)
XLA Ops:
  0.0 62.6 %layer.1 = bf16[256,2048]{1,0:T(8,128)(2,1)S(1)} custom-call(bf16[1024,512]{1,0:T(8,128)(2,1)} %tok_hbm.1, bf16[2048,256]{1,0:T(8,128)(2,1)} %wq_hbm.1, bf16[2048,256]{1,0:T(8,128)(2,1)} %wk_hbm.1, bf16[2048,256]{1,0:T(8,128)(2,1)} %wv_hbm.1, bf16[2048,256]{1,0:T(8,128)(2,1)} %wdg_hbm.1, bf16[2048,256]{1,0:T(8,128)(2,1)} %wgv_hbm.1, ...), custom_call_target="tpu_custom_call" | custom-call | flops 20000000000 | bytes 20000000 | tf_op jit(solution)/shard_map/layer/pallas_call | solution.py:780
  62.6 1.0 %copy.19 = bf16[256,2048]{1,0:T(8,128)(2,1)} copy(bf16[256,2048]{1,0:T(8,128)(2,1)S(1)} %layer.1) | data formatting | bytes 2097152
